TPU v7x, 128 devices: a whole 4x4x4 slice. The times are simulated.
128 devices in a mesh: rep: 2 (over z_hi), fs: 32 (over z_lo, y, x), tp: 2 (over core).
Axes of the slice: x: 4, y: 4, z: 4 (z_hi: 2, z_lo: 2; z = z_hi * 2 + z_lo), core: 2. Of those that a mesh axis runs over, the one named last changes fastest.
Arguments:
- tokens: bfloat16 [64, 256, 1024], P(('rep', 'fs'), None, 'tp'), may hold values from -6 to 6
- pre_gain: float32 [1024], replicated, may hold values from 0.1 to 1.9
- first_gate: bfloat16 [1024, 2560], P('fs', 'tp'), may hold values from -0.1875 to 0.1875
- first_up: bfloat16 [1024, 2560], P('fs', 'tp'), may hold values from -0.1875 to 0.1875
- first_down: bfloat16 [2560, 1024], P('tp', 'fs'), may hold values from -0.125 to 0.125
- mix_gain: float32 [1024], P('tp'), may hold values from 0.1 to 1.9
- pool_weight: bfloat16 [4, 256, 256], P('tp', None, 'fs'), may hold values from -0.375 to 0.375
- pool_scale: float32 [1024], P('tp'), may hold values from 0.1 to 1.9
- post_gain: float32 [1024], replicated, may hold values from 0.1 to 1.9
- second_gate: bfloat16 [1024, 2560], P('fs', 'tp'), may hold values from -0.1875 to 0.1875
- second_up: bfloat16 [1024, 2560], P('fs', 'tp'), may hold values from -0.1875 to 0.1875
- second_down: bfloat16 [2560, 1024], P('tp', 'fs'), may hold values from -0.125 to 0.125
Outputs:
- layer_out: bfloat16 [64, 256, 1024], P(('rep', 'fs'), None, 'tp')
All inputs are finite; a program needn't handle non-finite values.
Results may differ from a plain program's by a relative error of at most 0.015.
Values may be sent and summed in bfloat16 or wider, within the bound.
A program may use at most 64 MiB of HBM per device.

v0:
```python
import functools

import jax
import jax.numpy as jnp
from jax import lax
from jax.experimental import pallas as pl
from jax.experimental.pallas import tpu as pltpu
from jax.sharding import PartitionSpec as P

D = 1024
GROUPS = 4


epsilon = 1e-06


def taken_in(shard, axis, dim, take_in, carry):
    whole = jax.tree.map(lambda part: lax.all_gather(part, axis, axis=dim, tiled=True), shard)
    return take_in(carry, whole, jnp.int32(0))


def over_all(shard, axis, dim, block):
    whole = lax.all_gather(shard, axis, axis=dim, tiled=True)
    return block(whole, jnp.int32(0))


def normalize(values, gain_vec):
    floats = values.astype(jnp.float32)
    scaled = floats * lax.rsqrt(jnp.mean(floats * floats, axis=-1, keepdims=True) + epsilon)
    return (scaled * gain_vec.astype(jnp.float32)).astype(jnp.bfloat16)


def half_step(local_part, gain_vec, gate_w, up_w, down_w):
    gathered = lax.all_gather(local_part, "tp", axis=2, tiled=True)
    seq_count, seq_length, full_width = gathered.shape
    normed = normalize(gathered.reshape(seq_count * seq_length, full_width), gain_vec)
    zero_init = jnp.zeros((normed.shape[0], gate_w.shape[1]), jnp.float32)

    def add_rows(running, block_rows, offset):
        columns = lax.dynamic_slice_in_dim(normed, offset, block_rows.shape[0], 1)
        return running + jnp.dot(columns, block_rows, preferred_element_type=jnp.float32)

    gate_sum = taken_in(gate_w, "fs", 0, add_rows, zero_init)
    up_sum = taken_in(up_w, "fs", 0, add_rows, zero_init)
    hidden = (jax.nn.silu(gate_sum) * up_sum).astype(jnp.bfloat16)

    def project(block_cols, offset):
        return jnp.dot(hidden, block_cols, preferred_element_type=jnp.float32)

    partial_value = over_all(down_w, "fs", 1, project)
    own_part = lax.psum_scatter(
        partial_value.astype(jnp.bfloat16), "tp", scatter_dimension=1, tiled=True
    ).astype(jnp.float32)
    return own_part.reshape(seq_count, seq_length, own_part.shape[1])


def trailing(grouped, windows, widest):
    seq_length = grouped.shape[1]
    running = jnp.zeros_like(grouped)
    for back_step in range(widest):
        moved = jnp.pad(grouped, ((0, 0), (back_step, 0), (0, 0), (0, 0)))[:, :seq_length]
        running = running + jnp.where(back_step < windows[None, None, :, None], moved, 0.0)
    positions = jnp.arange(seq_length, dtype=jnp.int32)
    counts = jnp.minimum(positions[:, None] + 1, windows[None, :]).astype(jnp.float32)
    return running / counts[None, :, :, None]


def pool_mix(local_part, mix_gain, pool_weight, pool_scale):
    floats = local_part.astype(jnp.float32)
    squares = lax.psum(jnp.sum(floats * floats, axis=-1).astype(jnp.bfloat16), "tp").astype(
        jnp.float32
    )
    normed = (
        floats * lax.rsqrt(squares[..., None] / D + epsilon) * mix_gain.astype(jnp.float32)
    ).astype(jnp.bfloat16)
    seq_count, seq_length, part_width = local_part.shape
    groups_here = pool_weight.shape[0]
    group_width = pool_weight.shape[1]
    grouped = normed.astype(jnp.float32).reshape(seq_count, seq_length, groups_here, group_width)
    group_ids = lax.axis_index("tp") * groups_here + jnp.arange(groups_here, dtype=jnp.int32)
    windows = 2 ** (group_ids + 1)
    pooled = trailing(grouped, windows, 2**GROUPS)
    diff = (pooled - grouped).astype(jnp.bfloat16)

    def mix_cols(block_cols, offset):
        return jnp.einsum("bsgc,gcd->bsgd", diff, block_cols, preferred_element_type=jnp.float32)

    mixed = over_all(pool_weight, "fs", 2, mix_cols)
    mixed = mixed.reshape(seq_count, seq_length, part_width)
    return (floats + mixed * pool_scale.astype(jnp.float32)).astype(jnp.bfloat16)


def local(
    tokens,
    pre_gain,
    first_gate,
    first_up,
    first_down,
    mix_gain,
    pool_weight,
    pool_scale,
    post_gain,
    second_gate,
    second_up,
    second_down,
):
    first_out = half_step(tokens, pre_gain, first_gate, first_up, first_down)
    after_first = (tokens.astype(jnp.float32) + 0.5 * first_out).astype(jnp.bfloat16)
    after_mix = pool_mix(after_first, mix_gain, pool_weight, pool_scale)
    second_out = half_step(after_mix, post_gain, second_gate, second_up, second_down)
    return (after_mix.astype(jnp.float32) + 0.5 * second_out).astype(jnp.bfloat16)


F32 = jnp.float32
BF16 = jnp.bfloat16


def layer_kernel(
    nz, tok_ref, pre_ref, mixg_ref, scale_ref, post_ref, pw_ref,
    g1_ref, u1_ref, d1_ref, g2_ref, u2_ref, d2_ref, out_ref,
    GU, DW, PW, T, N, ACC, H, PS, PR, S, R, SQ, TG, TL, tg_s,
    sw_s, sw_r, loc, zs, zr, ts, tr, cs, cr, os_, or_, ps_, pr_, qs, qr,
):
    r = lax.axis_index("rep")
    f = lax.axis_index("fs")
    t = lax.axis_index("tp")
    x = lax.rem(r, 2)
    y = lax.rem(f, 2)
    z = f // 2
    rx = r + 1 - 2 * x
    fy = f + 1 - 2 * y
    me = 2 * x + y
    other = 1 - t

    def dev(rr, ff, tt):
        return {"rep": rr, "fs": ff, "tp": tt}

    quad = (dev(rx, f, t), dev(r, fy, t), dev(rx, fy, t))
    quad_idx = (2 * (1 - x) + y, 2 * x + (1 - y), 2 * (1 - x) + (1 - y))
    mate = dev(r, f, other)
    above = dev(r, f + 2, t)
    below = dev(r, f - 2, t)
    has_above = z < nz - 1
    has_below = z > 0

    barrier = pltpu.get_barrier_semaphore()
    for peer in quad + (mate,):
        pl.semaphore_signal(barrier, inc=1, device_id=peer, device_id_type=pl.DeviceIdType.MESH)

    @pl.when(has_above)
    def _():
        pl.semaphore_signal(barrier, inc=1, device_id=above, device_id_type=pl.DeviceIdType.MESH)

    @pl.when(has_below)
    def _():
        pl.semaphore_signal(barrier, inc=1, device_id=below, device_id_type=pl.DeviceIdType.MESH)

    def remote(src, dst, ss, rs, to):
        return pltpu.make_async_remote_copy(
            src_ref=src, dst_ref=dst, send_sem=ss, recv_sem=rs,
            device_id=to, device_id_type=pl.DeviceIdType.MESH,
        )

    rows, half = tok_ref.shape
    depth = g1_ref.shape[0]
    main = (g1_ref.shape[1] // 512) * 128
    rest = g1_ref.shape[1] // 4 - main
    big = GU.shape[-1]
    cw = d1_ref.shape[1]
    weights = ((g1_ref, u1_ref, TL.at[0], d1_ref), (g2_ref, u2_ref, TL.at[1], d2_ref))

    def pieces(b, q):
        g, u, tl, d = weights[b]
        lanes = pl.ds(pl.multiple_of(q * main, 128), main)
        ends = pl.ds(pl.multiple_of(q * 2 * rest, 128), 2 * rest)
        deep = pl.ds(pl.multiple_of(y * depth, 128), depth)
        rows_main = pl.ds(pl.multiple_of(q * main, 128), main)
        rows_rest = pl.ds(pl.multiple_of(4 * main + q * rest, 16), rest)
        return (
            (g.at[:, lanes], GU.at[b, z, deep, 0:main]),
            (u.at[:, lanes], GU.at[b, z, deep, main:2 * main]),
            (tl.at[:, ends], GU.at[b, z, deep, 2 * main:big]),
            (d.at[rows_main, :], DW.at[b, z, y, 0:main, :]),
            (d.at[rows_rest, :], DW.at[b, z, y, main:main + rest, :]),
        )

    def tail_loads(b):
        return [
            pltpu.make_async_copy(weights[b][i].at[:, 4 * main:], TG.at[b, i], tg_s.at[b, i])
            for i in range(2)
        ]

    def tail_make(b):
        for c in tail_loads(b):
            c.wait()
        for q in range(4):
            cut = slice(q * rest, (q + 1) * rest)
            TL[b, :, q * 2 * rest:(q + 1) * 2 * rest] = jnp.concatenate(
                [TG[b, 0, :, cut], TG[b, 1, :, cut]], axis=1
            )

    def own_copies(b):
        found = [pltpu.make_async_copy(s, d, loc.at[b, i]) for i, (s, d) in enumerate(pieces(b, me))]
        if b == 0:
            found.append(pltpu.make_async_copy(pw_ref, PW.at[z, y], loc.at[b, 5]))
        return found

    def swaps(b):
        found = [
            remote(s, d, sw_s.at[b, i], sw_r.at[b, i], quad[1])
            for i, (s, d) in enumerate(pieces(b, quad_idx[1]))
        ]
        if b == 0:
            found.append(remote(pw_ref, PW.at[z, y], sw_s.at[b, 5], sw_r.at[b, 5], quad[1]))
        return found

    kinds = (GU, DW)

    def z_up(b, k, kind):
        p = jnp.maximum(z - k, 0)
        ref = PW.at[p] if kind == 2 else kinds[kind].at[b, p]
        return remote(ref, ref, zs.at[0, b, k, kind], zr.at[0, b, k, kind], above)

    def z_down(b, k, kind):
        p = jnp.minimum(z + k, nz - 1)
        ref = PW.at[p] if kind == 2 else kinds[kind].at[b, p]
        return remote(ref, ref, zs.at[1, b, k, kind], zr.at[1, b, k, kind], below)

    def can_up(k):
        return jnp.logical_and(has_above, z - k >= 0)

    def can_down(k):
        return jnp.logical_and(has_below, z + k <= nz - 1)

    def z_send(b, k, kind):
        @pl.when(can_up(k))
        def _():
            z_up(b, k, kind).start()

        @pl.when(can_down(k))
        def _():
            z_down(b, k, kind).start()

    def z_sent(b, k, kind):
        @pl.when(can_up(k))
        def _():
            z_up(b, k, kind).wait_send()

        @pl.when(can_down(k))
        def _():
            z_down(b, k, kind).wait_send()

    def z_take(b, k, kind):
        @pl.when(z - 1 - k >= 0)
        def _():
            z_up(b, k, kind).wait_recv()

        @pl.when(z + 1 + k <= nz - 1)
        def _():
            z_down(b, k, kind).wait_recv()

        if k + 1 < nz - 1:
            z_send(b, k + 1, kind)

    def tok_sends(b):
        mine = T.at[b, me, t]
        return [remote(mine, mine, ts.at[b, j], tr.at[b, j], quad[j]) for j in range(3)]

    def mate_own(b):
        mine = T.at[b, me, t]
        return remote(mine, mine, os_.at[b], or_.at[b], mate)

    def mate_pass(b, j):
        got = T.at[b, quad_idx[j], t]
        return remote(got, got, cs.at[b, j], cr.at[b, j], mate)

    def order(i):
        m = jnp.minimum(z, nz - 1 - z)
        near = z - (i + 1) // 2 if i % 2 else z + i // 2
        far = jnp.where(2 * z < nz - 1, i, nz - 1 - i)
        return jnp.where(i <= 2 * m, near, far)

    def norm_block(b, q, gain_ref):
        parts = [T[b, q, c].astype(F32) for c in range(2)]
        total = sum(jnp.sum(v * v, axis=-1, keepdims=True) for v in parts)
        inv = lax.rsqrt(total / (2 * half) + epsilon)
        step = N.shape[2]
        for c in range(2):
            done = (parts[c] * inv * gain_ref[0:1, c * half:(c + 1) * half]).astype(BF16)
            for i in range(half // step):
                N[c * (half // step) + i, pl.ds(pl.multiple_of(q * rows, 128), rows), :] = done[:, i * step:(i + 1) * step]

    def gate_up(b, i):
        p = order(i)

        @pl.loop(0, 4)
        def _(q):
            at = pl.ds(pl.multiple_of(q * rows, 128), rows)
            value = jnp.dot(N[p, at, :], GU[b, p], preferred_element_type=F32)
            if i == 0:
                ACC[at, :] = value
            else:
                ACC[at, :] += value

    turn = (quad_idx[2], quad_idx[0], quad_idx[1], me)
    turn_peer = (2, 0, 1)

    def rows_of(q):
        return pl.ds(pl.multiple_of(q * rows, 128), rows)

    def hidden_of(q):
        at = rows_of(q)
        gate = ACC[at, 0:main]
        up = ACC[at, main:2 * main]
        H[at, 0:main] = (jax.nn.silu(gate) * up).astype(BF16)
        last = ACC[at, 2 * main:big]
        H[at, main:main + rest] = (jax.nn.silu(last[:, :rest]) * last[:, rest:]).astype(BF16)

    def half_send(b, i):
        span = pl.ds(other * (nz // 2), nz // 2)
        q = turn[i]
        return remote(PS.at[b, q, span], PR.at[b, q], ps_.at[b, i], pr_.at[b, i], mate)

    def half_sends(b):
        return [half_send(b, i) for i in range(4)]

    def down(b, i):
        q = turn[i]
        for p in range(nz):
            wide = jnp.concatenate([DW[b, p, 0], DW[b, p, 1]], axis=1)
            PS[b, q, p] = jnp.dot(H[rows_of(q), :], wide, preferred_element_type=F32).astype(BF16)
        half_send(b, i).start()

    def quad_send(b, j):
        return remote(S.at[b, quad_idx[j]], R.at[b, j], qs.at[b, j], qr.at[b, j], quad[j])

    def quad_sends(b):
        return [quad_send(b, j) for j in range(3)]

    def sum_half(b, i):
        half_send(b, i).wait_recv()
        q = turn[i]
        for k in range(nz // 2):
            mine = PS[b, q, t * (nz // 2) + k].astype(F32)
            S[b, q, :, k * 2 * cw:(k + 1) * 2 * cw] = (mine + PR[b, q, k].astype(F32)).astype(BF16)
        if i < 3:
            quad_send(b, turn_peer[i]).start()

    def project(b, prepare):
        for i in range(4):
            prepare(turn[i])
            hidden_of(turn[i])
            down(b, i)
            if i:
                sum_half(b, i - 1)
        sum_half(b, 3)

    def chunk(b, i, q, fresh):
        p = order(i)
        value = jnp.dot(N[p, rows_of(q), :], GU[b, p], preferred_element_type=F32)
        if fresh:
            ACC[rows_of(q), :] = value
        else:
            ACC[rows_of(q), :] += value

    def collect(b):
        for send in quad_sends(b):
            send.wait_recv()
        total = S[b, me].astype(F32)
        for j in (2, 0, 1):
            total = total + R[b, j].astype(F32)
        return total

    for b in range(2):
        for c in tail_loads(b):
            c.start()
    T[0, me, t] = tok_ref[...]
    for b in range(2):
        tail_make(b)
    for c in own_copies(0):
        c.start()
    pl.semaphore_wait(
        barrier, 4 + jnp.minimum(z, 1) + jnp.minimum(nz - 1 - z, 1)
    )

    for c in swaps(0)[:5]:
        c.start()
    for j in (0, 2, 1):
        tok_sends(0)[j].start()
    mate_own(0).start()
    swaps(0)[5].start()
    for c in own_copies(1):
        c.start()
    for c in swaps(1):
        c.start()
    for i, c in enumerate(own_copies(0)):
        c.wait()
    for i in (0, 1, 2):
        swaps(0)[i].wait_recv()
    z_send(0, 0, 0)
    for i in (3, 4):
        swaps(0)[i].wait_recv()
    z_send(0, 0, 1)
    mate_own(0).wait_recv()
    norm_block(0, me, pre_ref)
    for j in (0, 2, 1):
        tok_sends(0)[j].wait_recv()
        mate_pass(0, j).start()
    for j in (0, 2, 1):
        mate_pass(0, j).wait_recv()
        norm_block(0, quad_idx[j], pre_ref)
    swaps(0)[5].wait_recv()
    gate_up(0, 0)
    for k in range(nz - 1):
        z_take(0, k, 0)
        gate_up(0, k + 1)
        z_take(0, k, 1)
        if k == 0:
            z_send(0, 0, 2)
        else:
            z_take(0, k - 1, 2)
        if k == max(nz - 3, 0):
            for c in own_copies(1):
                c.wait()
            for c in swaps(1):
                c.wait_recv()
            z_send(1, 0, 0)
            z_send(1, 0, 1)
    project(0, lambda q: None)
    z_take(0, nz - 2, 2)
    z_take(1, 0, 0)
    z_take(1, 0, 1)
    first = collect(0)
    after_first = (tok_ref[...].astype(F32) + 0.5 * first).astype(BF16).astype(F32)
    square = after_first * after_first
    SQ[0] = sum(square[:, i * 128:(i + 1) * 128] for i in range(half // 128))
    swap_sq = remote(SQ.at[0], SQ.at[1], os_.at[2], or_.at[2], mate)
    swap_sq.start()
    swap_sq.wait_recv()
    total = jnp.sum(SQ[0] + SQ[1], axis=-1, keepdims=True)
    h = (after_first * lax.rsqrt(total / (2 * half) + epsilon) * mixg_ref[0:1, :]).astype(BF16).astype(F32)
    position = lax.broadcasted_iota(jnp.int32, (rows, 128), 0)
    groups_here = pw_ref.shape[0]
    width = half // groups_here

    def shifted(v, by):
        place = lax.broadcasted_iota(jnp.int32, v.shape, 0)
        return jnp.where(place >= by, pltpu.roll(v, by, 0), 0.0)

    for g in range(groups_here):
        hg = h[:, g * width:(g + 1) * width]
        run = hg + shifted(hg, 1)
        window = 2
        found = run
        number = t * groups_here + g
        reached = jnp.int32(2)
        for level in range(1, GROUPS):
            run = run + shifted(run, window)
            window = window * 2
            found = jnp.where(number >= level, run, found)
            reached = jnp.where(number >= level, window, reached)
        counts = jnp.minimum(lax.broadcasted_iota(jnp.int32, (rows, width), 0) + 1, reached).astype(F32)
        diff = (found / counts - hg).astype(BF16)
        turned = jnp.concatenate([PW[i // 2, i % 2, g] for i in range(2 * nz)], axis=0)
        mixed = lax.dot_general(diff, turned, (((1,), (1,)), ((), ())), preferred_element_type=F32)
        at = slice(g * width, (g + 1) * width)
        T[1, me, t, :, at] = (after_first[:, at] + scale_ref[0:1, at] * mixed).astype(BF16)
    for j in (0, 2, 1):
        tok_sends(1)[j].start()
    mate_own(1).start()
    z_take(1, 1, 0)
    z_take(1, 1, 1)
    mate_own(1).wait_recv()
    norm_block(1, me, post_ref)
    for i in range(nz - 1):
        chunk(1, i, me, i == 0)
    for j in (0, 2, 1):
        tok_sends(1)[j].wait_recv()
        mate_pass(1, j).start()
    for j in (0, 2, 1):
        mate_pass(1, j).wait_recv()
        norm_block(1, quad_idx[j], post_ref)
        for i in range(nz - 1):
            chunk(1, i, quad_idx[j], i == 0)
    for k in range(2, nz - 1):
        z_take(1, k, 0)
        z_take(1, k, 1)
    project(1, lambda q: chunk(1, nz - 1, q, False))
    out_ref[...] = (T[1, me, t].astype(F32) + 0.5 * collect(1)).astype(BF16)

    for b in range(2):
        for c in swaps(b) + tok_sends(b) + [mate_own(b)] + [mate_pass(b, j) for j in range(3)]:
            c.wait_send()
        for c in half_sends(b) + quad_sends(b):
            c.wait_send()
        for k in range(nz - 1):
            for kind in range(3 if b == 0 else 2):
                z_sent(b, k, kind)
    swap_sq.wait_send()


def fused(
    fs, tokens, pre_gain, first_gate, first_up, first_down, mix_gain, pool_weight,
    pool_scale, post_gain, second_gate, second_up, second_down,
):
    nz = fs // 2
    _, rows, half = tokens.shape
    depth, hid = first_gate.shape
    cw = first_down.shape[1]
    main = (hid // 512) * 128
    rest = hid // 4 - main
    groups, width, out_cols = pool_weight.shape

    vmem = pl.BlockSpec(memory_space=pltpu.VMEM)
    anyw = pl.BlockSpec(memory_space=pl.ANY)
    dma = pltpu.SemaphoreType.DMA
    big = 2 * main + 2 * rest
    steps = nz - 1
    out = pl.pallas_call(
        functools.partial(layer_kernel, nz),
        out_shape=jax.ShapeDtypeStruct((rows, half), BF16),
        in_specs=[vmem] * 6 + [anyw] * 6,
        out_specs=vmem,
        scratch_shapes=[
            pltpu.VMEM((2, nz, 2 * depth, big), BF16),
            pltpu.VMEM((2, nz, 2, main + rest, cw), BF16),
            pltpu.VMEM((nz, 2, groups, out_cols, width), BF16),
            pltpu.VMEM((2, 4, 2, rows, half), BF16),
            pltpu.VMEM((nz, 4 * rows, 2 * depth), BF16),
            pltpu.VMEM((4 * rows, big), F32),
            pltpu.VMEM((4 * rows, main + rest), BF16),
            pltpu.VMEM((2, 4, nz, rows, 2 * cw), BF16),
            pltpu.VMEM((2, 4, nz // 2, rows, 2 * cw), BF16),
            pltpu.VMEM((2, 4, rows, half), BF16),
            pltpu.VMEM((2, 3, rows, half), BF16),
            pltpu.VMEM((2, rows, 128), F32),
            pltpu.VMEM((2, 2, depth, 4 * rest), BF16),
            pltpu.VMEM((2, depth, 8 * rest), BF16),
            dma((2, 2)),
            dma((2, 6)), dma((2, 6)), dma((2, 6)),
            dma((2, 2, steps, 3)), dma((2, 2, steps, 3)),
            dma((2, 3)), dma((2, 3)), dma((2, 3)), dma((2, 3)),
            dma((3,)), dma((3,)), dma((2, 4)), dma((2, 4)), dma((2, 3)), dma((2, 3)),
        ],
        compiler_params=pltpu.CompilerParams(
            collective_id=0, has_side_effects=True, vmem_limit_bytes=60 * 1024 * 1024
        ),
    )(
        tokens.reshape(rows, half), pre_gain.reshape(1, -1), mix_gain.reshape(1, -1),
        pool_scale.reshape(1, -1), post_gain.reshape(1, -1), jnp.swapaxes(pool_weight, 1, 2),
        first_gate, first_up, first_down, second_gate, second_up, second_down,
    )
    return out.reshape(tokens.shape)


def whole_tiles(mesh, args):
    reps, fs, tp = (mesh.shape[name] for name in ("rep", "fs", "tp"))
    depth = args[2].shape[0] // fs
    hid = args[2].shape[1] // tp
    return (
        tp == 2 and reps % 2 == 0 and fs % 8 == 0 and depth % 128 == 0
        and args[0].shape[0] == reps * fs and args[4].shape[1] // fs == depth
        and hid % 512 == 256 and args[6].shape[2] % (fs * 16) == 0
    )


def solution(mesh):
    placed = (
        P(("rep", "fs"), None, "tp"),
        P(),
        P("fs", "tp"),
        P("fs", "tp"),
        P("tp", "fs"),
        P("tp"),
        P("tp", None, "fs"),
        P("tp"),
        P(),
        P("fs", "tp"),
        P("fs", "tp"),
        P("tp", "fs"),
    )
    def layer(*args):
        body = functools.partial(fused, mesh.shape["fs"]) if whole_tiles(mesh, args) else local
        return jax.shard_map(
            body, mesh=mesh, in_specs=placed, out_specs=P(("rep", "fs"), None, "tp"), check_vma=False
        )(*args)

    return layer
```

profile of v0, /device:TPU:1, one launch (start us, length us, event | category | flops | bytes accessed | tf_op | source)
XLA Modules:
  0.0 984.1 jit_solution(10474154368155014482)
XLA Ops:
  6.5 0.7 all-gather.7.cloned.1.call-update
  7.3 0.7 all-gather.11.cloned.1.call-update
  8.1 0.7 all-gather.9.cloned.1.call-update
  8.8 3.4 all_gather.27
  12.2 0.2 fusion.2
  12.4 131.5 %all-gather.7.cloned.1.call-done = bf16[1024,1280]{1,0:T(8,128)(2,1)} async-done(((bf16[32,1280]{1,0:T(8,128)(2,1)}), bf16[1024,1280]{1,0:T(8,128)(2,1)}) %all-gather.7.cloned.1.call-update) | async-done | bytes 2621456 | tf_op jit(solution)/shard_map/all_gather | solution.py:18
  143.9 2.6 fusion.55
  146.6 152.8 %all-gather.11.cloned.1.call-done = bf16[1280,1024]{0,1:T(8,128)(2,1)} async-done(((bf16[1280,32]{0,1:T(8,128)(2,1)}), bf16[1280,1024]{0,1:T(8,128)(2,1)}) %all-gather.11.cloned.1.call-update) | async-done | bytes 2621456 | tf_op jit(solution)/shard_map/all_gather | solution.py:23
  299.3 155.2 %all-gather.9.cloned.1.call-done = bf16[1024,1280]{1,0:T(8,128)(2,1)} async-done(((bf16[32,1280]{1,0:T(8,128)(2,1)}), bf16[1024,1280]{1,0:T(8,128)(2,1)}) %all-gather.9.cloned.1.call-update) | async-done | bytes 2621456 | tf_op jit(solution)/shard_map/all_gather | solution.py:18
  454.5 5.0 convolution_convert_fusion.1
  459.5 0.0 all-gather.13.cloned.1.call-start
  459.6 0.5 all-gather.13.cloned.1.call-update
  460.2 0.5 all-gather.15.cloned.1.call-update
  460.7 0.7 all-gather.17.cloned.1.call-update
  461.4 0.0 reduce-scatter.5.cloned.1.call-start
  461.7 68.0 %all_gather.31 = bf16[2,256,256]{1,2,0:T(8,128)(2,1)S(1)} all-gather(bf16[2,256,8]{1,2,0:T(8,128)(2,1)S(1)} %copy-done.4), channel_id=1, replica_groups=mesh['rep'=2,'fs'=32,'tp'=2] {'fs'}, dimensions={2}, use_global_device_ids=true | all-gather | bytes 270336 | tf_op jit(solution)/shard_map/all_gather | solution.py:23
  529.7 0.1 minimum_convert_fusion
  529.8 1.1 fusion.40
  530.9 38.9 %psum.7 = bf16[1,256]{1,0:T(2,128)(2,1)S(1)} all-reduce(bf16[1,256]{1,0:T(2,128)(2,1)S(1)} %convert_element_type.125), channel_id=1, replica_groups=mesh['rep'=2,'fs'=32,'tp'=2] {'tp'}, use_global_device_ids=true, to_apply=%region_3.4 | all-reduce | flops 256 | bytes 1024 | tf_op jit(solution)/shard_map/psum | solution.py:70
  569.8 1.1 fusion.46
  571.0 1.8 fusion.47
  572.8 0.2 copy.31
  573.0 0.1 fusion.43
  573.1 2.2 all_gather.32
  575.3 0.2 fusion.5
  575.5 51.3 %all-gather.13.cloned.1.call-done = bf16[1024,1280]{1,0:T(8,128)(2,1)} async-done(((bf16[32,1280]{1,0:T(8,128)(2,1)}), bf16[1024,1280]{1,0:T(8,128)(2,1)}) %all-gather.13.cloned.1.call-update) | async-done | bytes 2621456 | tf_op jit(solution)/shard_map/all_gather | solution.py:18
  626.9 2.6 fusion.51
  629.5 152.5 %all-gather.15.cloned.1.call-done = bf16[1024,1280]{1,0:T(8,128)(2,1)} async-done(((bf16[32,1280]{1,0:T(8,128)(2,1)}), bf16[1024,1280]{1,0:T(8,128)(2,1)}) %all-gather.15.cloned.1.call-update) | async-done | bytes 2621456 | tf_op jit(solution)/shard_map/all_gather | solution.py:18
  782.0 155.5 %all-gather.17.cloned.1.call-done = bf16[1280,1024]{0,1:T(8,128)(2,1)} async-done(((bf16[1280,32]{0,1:T(8,128)(2,1)}), bf16[1280,1024]{0,1:T(8,128)(2,1)}) %all-gather.17.cloned.1.call-update) | async-done | bytes 2621456 | tf_op jit(solution)/shard_map/all_gather | solution.py:23
  937.5 4.9 convolution_convert_fusion
  942.5 33.1 %reduce-scatter.5.cloned.1.call-done = bf16[256,512]{1,0:T(8,128)(2,1)} async-done(((bf16[256,1024]{1,0:T(8,128)(2,1)}), bf16[256,512]{1,0:T(8,128)(2,1)}) %reduce-scatter.5.cloned.1.call-update) | async-done | bytes 262160 | tf_op jit(solution)/shard_map/reduce_scatter | solution.py:51
  975.5 1.7 fusion.44
  (38 shorter events, 0.5 us)
Async XLA Ops:
  6.5 137.3 %all-gather.7.cloned.1.call-start = ((), (), s32[]{:S(2)}) async-start(), calls=%async_computation.2 | async-start | bytes 2703360 | tf_op jit(solution)/shard_map/all_gather | solution.py:18
  7.3 292.1 %all-gather.11.cloned.1.call-start = ((), (), s32[]{:S(2)}) async-start(), calls=%async_computation.4 | async-start | bytes 2703360 | tf_op jit(solution)/shard_map/all_gather | solution.py:23
  8.0 446.5 %all-gather.9.cloned.1.call-start = ((), (), s32[]{:S(2)}) async-start(), calls=%async_computation.3 | async-start | bytes 2703360 | tf_op jit(solution)/shard_map/all_gather | solution.py:18
  8.7 521.0 %reduce-scatter.3.cloned.1.call-start = ((), (), s32[]{:S(2)}) async-start(), calls=%async_computation.5 | async-start | bytes 786432 | tf_op jit(solution)/shard_map/reduce_scatter | solution.py:51
  12.2 442.3 %copy-start.2 = (f32[1024]{0:T(1024)S(1)}, f32[1024]{0:T(1024)}, u32[]{:S(2)}) copy-start(f32[1024]{0:T(1024)} %param.13) | copy-start | bytes 12292
  146.5 315.2 %copy-start.4 = (bf16[2,256,8]{1,2,0:T(8,128)(2,1)S(1)}, bf16[2,256,8]{1,2,0:T(8,128)(2,1)}, u32[]{:S(2)}) copy-start(bf16[2,256,8]{1,2,0:T(8,128)(2,1)} %param.18) | copy-start | bytes 24580
  146.5 383.3 %copy-start = (bf16[1,256,512]{2,1,0:T(8,128)(2,1)S(1)}, bf16[1,256,512]{2,1,0:T(8,128)(2,1)}, u32[]{:S(2)}) copy-start(bf16[1,256,512]{2,1,0:T(8,128)(2,1)} %param.12) | copy-start | bytes 786436
  146.5 423.3 %copy-start.5 = (f32[512]{0:T(512)S(1)}, f32[512]{0:T(512)}, u32[]{:S(2)}) copy-start(f32[512]{0:T(512)} %param.17) | copy-start | bytes 6148
  459.5 167.3 %all-gather.13.cloned.1.call-start = ((), (), s32[]{:S(2)}) async-start(), calls=%async_computation.6 | async-start | bytes 2703360 | tf_op jit(solution)/shard_map/all_gather | solution.py:18
  460.1 321.9 %all-gather.15.cloned.1.call-start = ((), (), s32[]{:S(2)}) async-start(), calls=%async_computation.7 | async-start | bytes 2703360 | tf_op jit(solution)/shard_map/all_gather | solution.py:18
  460.7 476.8 %all-gather.17.cloned.1.call-start = ((), (), s32[]{:S(2)}) async-start(), calls=%async_computation.8 | async-start | bytes 2703360 | tf_op jit(solution)/shard_map/all_gather | solution.py:23
  461.4 514.1 %reduce-scatter.5.cloned.1.call-start = ((), (), s32[]{:S(2)}) async-start(), calls=%async_computation.9 | async-start | bytes 786432 | tf_op jit(solution)/shard_map/reduce_scatter | solution.py:51
  571.0 2.0 copy-start.1
  571.0 2.0 copy-start.6
  572.8 54.1 %copy-start.3 = (f32[1024]{0:T(1024)S(1)}, f32[1024]{0:T(1024)}, u32[]{:S(2)}) copy-start(f32[1024]{0:T(1024)} %param.20) | copy-start | bytes 12292
Sparse Core Ops, SparseCore 0:
  9.0 134.8 all-gather.6
  145.5 153.7 all-gather.10
  301.0 153.4 all-gather.8
  459.6 33.0 reduce-scatter.2
  494.2 132.6 all-gather.12
  628.4 153.6 all-gather.14
  783.7 153.7 all-gather.16
  942.6 32.8 reduce-scatter.4
where the time goes:
time: 984 us
  waiting for transfers between devices  836 us (85%)
  blocking collectives  112 us (11%)
  matrix products  17 us (2%)
  between operations  13.7 us (1%)
    all_gather x4, waiting for transfers between devices, taken_in(): lax.all_gather(part, axis, axis=dim, tiled=True)  491 us
    all_gather x2, waiting for transfers between devices, over_all(): whole = lax.all_gather(shard, axis, axis=dim, tiled=True)  308 us
    all_gather x1, blocking collectives, over_all(): whole = lax.all_gather(shard, axis, axis=dim, tiled=True)  68 us
    psum x1, blocking collectives, pool_mix(): lax.psum(jnp.sum(floats * floats, axis=-1).astype(jnp.bfloat16), 'tp')  38.9 us
    reduce_scatter x2, waiting for transfers between devices, half_step(): lax.psum_scatter(partial_value.astype(jnp.bfloat16), 'tp', scatter_dimens...  33.1 us
  transfers between devices with their start and end apart: 8, of which 7 were waited for; matrix products, arithmetic and copies ran while one was open for 1% of the time, Pallas kernels for 0%

commit v1 on v0

v1 whole, which is shorter than its diff:
```python
import functools

import jax
import jax.numpy as jnp
from jax import lax
from jax.experimental import pallas as pl
from jax.experimental.pallas import tpu as pltpu
from jax.sharding import PartitionSpec as P

F32 = jnp.float32
BF16 = jnp.bfloat16
MESH = pl.DeviceIdType.MESH
GROUPS = 4
SIDE = 4
epsilon = 1e-06
NT = (((1,), (1,)), ((), ()))


def layer_kernel(
    tok_ref, pre_ref, mixg_ref, scale_ref, post_ref, pw_ref,
    g1_ref, u1_ref, d1_ref, g2_ref, u2_ref, d2_ref, out_ref,
    WS0, WS1, WB0, WB1, TB, N, ACC, H, PX, PR, PO, S, R, SQ,
    xs, xr, ys, yr, zs, zr, ts, tr, ms, mr, hs, hr, rs, rr, qs,
):
    rep = lax.axis_index("rep")
    fs = lax.axis_index("fs")
    t = lax.axis_index("tp")
    x = lax.rem(fs, SIDE)
    y = lax.rem(fs // SIDE, SIDE)
    low = fs // (SIDE * SIDE)
    z = 2 * rep + low
    other = 1 - t
    high = 1 - low

    def dev(dx, dy, dz, tt):
        xx = lax.rem(x + dx, SIDE)
        yy = lax.rem(y + dy, SIDE)
        zz = lax.rem(z + dz, SIDE)
        return {"rep": zz // 2, "fs": lax.rem(zz, 2) * (SIDE * SIDE) + yy * SIDE + xx, "tp": tt}

    mate = dev(0, 0, 0, other)
    along_x = {d: dev(d, 0, 0, t) for d in (1, 2, 3)}
    along_y = {d: dev(0, d, 0, t) for d in (1, 2, 3)}
    along_z = {d: dev(0, 0, d, t) for d in (1, 3)}
    peers = [mate] + list(along_x.values()) + list(along_y.values()) + list(along_z.values())

    barrier = pltpu.get_barrier_semaphore()
    for peer in peers:
        pl.semaphore_signal(barrier, inc=1, device_id=peer, device_id_type=MESH)

    def remote(src, dst, ss, sr, to):
        return pltpu.make_async_remote_copy(
            src_ref=src, dst_ref=dst, send_sem=ss, recv_sem=sr, device_id=to, device_id_type=MESH
        )

    rows, half = tok_ref.shape
    depth, hid = g1_ref.shape
    part = hid // 2
    piece = rows // 2
    step = half // SIDE
    weights = ((g1_ref, u1_ref, d1_ref), (g2_ref, u2_ref, d2_ref))
    WS = (WS0, WS1)
    WB = (WB0, WB1)
    axis = (along_x, along_y)
    ring = (along_y, along_x)
    place = (x, y)
    spot = (y, x)

    def slab(b, lo, a, c):
        return WB[b].at[lo, c, a] if b == 0 else WB[b].at[lo, a, c]

    def line(b, lo, c):
        return WB[b].at[lo, c] if b == 0 else WB[b].at[lo, :, c]

    def line_half(b, lo, c, k):
        cut = slice(2 * k, 2 * k + 2)
        return WB[b].at[lo, c, cut] if b == 0 else WB[b].at[lo, cut, c]

    def pack(b):
        for k in range(2):
            for i, w in enumerate(weights[b]):
                WS[b][k, :, i * part:(i + 1) * part] = w[:, k * part:(k + 1) * part]
            if b == 0:
                flat = pw_ref[...]
                for i in range(2):
                    WS[b][k, i * 16:(i + 1) * 16, 3 * part:] = flat[:, i * 128:(i + 1) * 128]
        mine = lax.rem(place[b], 2)
        if b == 0:
            WB[b][low, y, x] = WS[b][mine]
        else:
            WB[b][low, y, x] = WS[b][mine]

    def class_send(b, i):
        d = (1, 3, 2)[i]
        kind = lax.rem(place[b] + d, 2)
        return remote(WS[b].at[kind], slab(b, low, place[b], spot[b]), xs.at[b, i], xr.at[b, i], axis[b][d])

    def ring_send(b, i):
        c = spot[b]
        if i < 2:
            ref = line(b, low, c)
            return remote(ref, ref, ys.at[b, i], yr.at[b, i], ring[b][(1, 3)[i]])
        if i == 2:
            ref = line_half(b, low, lax.rem(c + 3, SIDE), 0)
            return remote(ref, ref, ys.at[b, i], yr.at[b, i], ring[b][1])
        ref = line_half(b, low, lax.rem(c + 1, SIDE), 1)
        return remote(ref, ref, ys.at[b, i], yr.at[b, i], ring[b][3])

    def deep_send(b, j, k):
        c = lax.rem(spot[b] + (0, 3, 1, 2)[j], SIDE)
        ref = line_half(b, low, c, k)
        return remote(ref, ref, zs.at[b, j, k], zr.at[b, j, k], along_z[(1, 3)[k]])

    def tok_send(b, i):
        src = TB.at[b, t, i * piece:(i + 1) * piece]
        dst = TB.at[b, t, rows + i * piece:rows + (i + 1) * piece]
        return remote(src, dst, ts.at[b, i], tr.at[b, i], axis[b][(1, 3)[i]])

    def mate_send(b, i):
        cut = slice(0, rows) if i == 2 else slice(rows + i * piece, rows + (i + 1) * piece)
        ref = TB.at[b, t, cut]
        return remote(ref, ref, ms.at[b, i], mr.at[b, i], mate)

    chunks = (slice(rows, 2 * rows), slice(0, rows))

    def half_send(b, i):
        return remote(PX.at[b, chunks[i]], PR.at[b, chunks[i]], hs.at[b, i], hr.at[b, i], mate)

    def back_send(b, i):
        cut = slice(i * piece, (i + 1) * piece)
        return remote(S.at[b, cut], R.at[b, cut], rs.at[b, i], rr.at[b, i], axis[b][(3, 1)[i]])

    def norm_rows(b, cut, gain_ref):
        parts = [TB[b, c, cut].astype(F32) for c in range(2)]
        total = sum(jnp.sum(v * v, axis=-1, keepdims=True) for v in parts)
        inv = lax.rsqrt(total / (2 * half) + epsilon)
        for c in range(2):
            N[c, cut] = (parts[c] * inv * gain_ref[0:1, c * half:(c + 1) * half]).astype(BF16)

    def gate_up(b, lo, fresh):
        wide = WB[b][lo, :, :, :, 0:2 * part].reshape(half, 2 * part)
        for cut in chunks:
            value = jnp.dot(N[lo, cut], wide, preferred_element_type=F32)
            if fresh:
                ACC[cut] = value
            else:
                ACC[cut] += value

    def hidden(cut):
        H[cut] = (jax.nn.silu(ACC[cut, 0:part]) * ACC[cut, part:2 * part]).astype(BF16)

    def down(b, cut, lo):
        tall = WB[b][lo, :, :, :, 2 * part:3 * part].reshape(half, part)
        return lax.dot_general(H[cut], tall, NT, preferred_element_type=F32)

    def project(b):
        for i, cut in enumerate(chunks):
            hidden(cut)
            PX[b, cut] = down(b, cut, other).astype(BF16)
            half_send(b, i).start()
            PO[cut] = down(b, cut, t)
        half_send(b, 0).wait_recv()
        S[b] = (PO[chunks[0]] + PR[b, chunks[0]].astype(F32)).astype(BF16)
        for i in range(2):
            back_send(b, i).start()
        half_send(b, 1).wait_recv()
        total = PO[chunks[1]] + PR[b, chunks[1]].astype(F32)
        for i in range(2):
            back_send(b, i).wait_recv()
        return total + R[b].astype(F32)

    def spread(b):
        for i in range(3):
            class_send(b, i).wait_recv()
        for i in range(2):
            ring_send(b, i).start()

    def relay(b):
        for k in range(2):
            deep_send(b, 0, k).start()
        for i in range(2):
            ring_send(b, i).wait_recv()
            ring_send(b, 2 + i).start()
            for k in range(2):
                deep_send(b, 1 + i, k).start()
        for k in range(2):
            ring_send(b, 2 + k).wait_recv()
            deep_send(b, 3, k).start()

    def deep_wait(b):
        for j in range(4):
            for k in range(2):
                deep_send(b, j, k).wait_recv()

    TB[0, t, 0:rows] = tok_ref[...]
    pack(0)
    pack(1)
    pl.semaphore_wait(barrier, len(peers))

    for i in range(3):
        class_send(0, i).start()
    for i in range(3):
        class_send(1, i).start()
    mate_send(0, 2).start()
    for i in range(2):
        tok_send(0, i).start()
    mate_send(0, 2).wait_recv()
    norm_rows(0, chunks[1], pre_ref)
    spread(0)
    for i in range(2):
        tok_send(0, i).wait_recv()
        mate_send(0, i).start()
    spread(1)
    for i in range(2):
        mate_send(0, i).wait_recv()
    norm_rows(0, chunks[0], pre_ref)
    relay(0)
    gate_up(0, low, True)
    relay(1)
    deep_wait(0)
    gate_up(0, high, False)
    first = project(0)

    after_first = (tok_ref[...].astype(F32) + 0.5 * first).astype(BF16).astype(F32)
    square = after_first * after_first
    SQ[0] = sum(square[:, i * 128:(i + 1) * 128] for i in range(half // 128))
    swap = remote(SQ.at[0], SQ.at[1], qs.at[0], qs.at[1], mate)
    swap.start()
    swap.wait_recv()
    total = jnp.sum(SQ[0] + SQ[1], axis=-1, keepdims=True)
    h = (after_first * lax.rsqrt(total / (2 * half) + epsilon) * mixg_ref[0:1, :]).astype(BF16).astype(F32)
    groups_here = 2
    width = half // groups_here

    def shifted(v, by):
        spot_ids = lax.broadcasted_iota(jnp.int32, v.shape, 0)
        return jnp.where(spot_ids >= by, pltpu.roll(v, by, 0), 0.0)

    maps = WB0[:, :, :, :, 3 * part:].reshape(2 * SIDE * SIDE, depth, 128).astype(F32)
    maps = maps.reshape(2 * SIDE * SIDE, 4, 8, 128)
    for g in range(groups_here):
        hg = h[:, g * width:(g + 1) * width]
        run = hg + shifted(hg, 1)
        window = 2
        found = run
        number = t * groups_here + g
        reached = jnp.int32(2)
        for level in range(1, GROUPS):
            run = run + shifted(run, window)
            window = window * 2
            found = jnp.where(number >= level, run, found)
            reached = jnp.where(number >= level, window, reached)
        counts = jnp.minimum(lax.broadcasted_iota(jnp.int32, (rows, width), 0) + 1, reached).astype(F32)
        diff = (found / counts - hg).astype(BF16)
        turned = jnp.concatenate(
            [maps[:, g].reshape(width, 128), maps[:, 2 + g].reshape(width, 128)], axis=1
        ).astype(BF16)
        mixed = lax.dot_general(diff, turned, NT, preferred_element_type=F32)
        at = slice(g * width, (g + 1) * width)
        TB[1, t, 0:rows, at] = (after_first[:, at] + scale_ref[0:1, at] * mixed).astype(BF16)

    for i in range(2):
        tok_send(1, i).start()
    mate_send(1, 2).start()
    mate_send(1, 2).wait_recv()
    norm_rows(1, chunks[1], post_ref)
    for i in range(2):
        tok_send(1, i).wait_recv()
        mate_send(1, i).start()
    for i in range(2):
        mate_send(1, i).wait_recv()
    norm_rows(1, chunks[0], post_ref)
    gate_up(1, low, True)
    deep_wait(1)
    gate_up(1, high, False)
    second = project(1)
    out_ref[...] = (TB[1, t, 0:rows].astype(F32) + 0.5 * second).astype(BF16)

    for b in range(2):
        sent = [class_send(b, i) for i in range(3)] + [ring_send(b, i) for i in range(4)]
        sent += [deep_send(b, j, k) for j in range(4) for k in range(2)]
        sent += [tok_send(b, i) for i in range(2)] + [mate_send(b, i) for i in range(3)]
        sent += [half_send(b, i) for i in range(2)] + [back_send(b, i) for i in range(2)]
        for c in sent:
            c.wait_send()
    swap.wait_send()


def fused(
    tokens, pre_gain, first_gate, first_up, first_down, mix_gain, pool_weight,
    pool_scale, post_gain, second_gate, second_up, second_down,
):
    _, rows, half = tokens.shape
    depth, hid = first_gate.shape
    part = hid // 2
    groups, width, out_cols = pool_weight.shape

    vmem = pl.BlockSpec(memory_space=pltpu.VMEM)
    dma = pltpu.SemaphoreType.DMA
    out = pl.pallas_call(
        layer_kernel,
        out_shape=jax.ShapeDtypeStruct((rows, half), BF16),
        in_specs=[vmem] * 12,
        out_specs=vmem,
        scratch_shapes=[
            pltpu.VMEM((2, depth, 3 * part + 128), BF16),
            pltpu.VMEM((2, depth, 3 * part), BF16),
            pltpu.VMEM((2, SIDE, SIDE, depth, 3 * part + 128), BF16),
            pltpu.VMEM((2, SIDE, SIDE, depth, 3 * part), BF16),
            pltpu.VMEM((2, 2, 2 * rows, half), BF16),
            pltpu.VMEM((2, 2 * rows, half), BF16),
            pltpu.VMEM((2 * rows, 2 * part), F32),
            pltpu.VMEM((2 * rows, part), BF16),
            pltpu.VMEM((2, 2 * rows, half), BF16),
            pltpu.VMEM((2, 2 * rows, half), BF16),
            pltpu.VMEM((2 * rows, half), F32),
            pltpu.VMEM((2, rows, half), BF16),
            pltpu.VMEM((2, rows, half), BF16),
            pltpu.VMEM((2, rows, 128), F32),
            dma((2, 3)), dma((2, 3)), dma((2, 4)), dma((2, 4)), dma((2, 4, 2)), dma((2, 4, 2)),
            dma((2, 2)), dma((2, 2)), dma((2, 3)), dma((2, 3)), dma((2, 2)), dma((2, 2)),
            dma((2, 2)), dma((2, 2)), dma((2,)),
        ],
        compiler_params=pltpu.CompilerParams(
            collective_id=0, has_side_effects=True, vmem_limit_bytes=60 * 1024 * 1024
        ),
    )(
        tokens.reshape(rows, half), pre_gain.reshape(1, -1), mix_gain.reshape(1, -1),
        pool_scale.reshape(1, -1), post_gain.reshape(1, -1),
        jnp.swapaxes(pool_weight, 1, 2).reshape(groups * out_cols, width),
        first_gate, first_up, first_down.T, second_gate, second_up, second_down.T,
    )
    return out.reshape(tokens.shape)


def solution(mesh):
    tok = P(("rep", "fs"), None, "tp")
    wide = P("fs", "tp")
    tall = P("tp", "fs")
    placed = (
        tok, P(), wide, wide, tall, P("tp"), P("tp", None, "fs"), P("tp"), P(), wide, wide, tall,
    )

    def layer(*args):
        return jax.shard_map(fused, mesh=mesh, in_specs=placed, out_specs=tok, check_vma=False)(*args)

    return layer
```

time: 984 us -> 78.6 us (0.08)
  waiting for transfers between devices: 836 us -> 0 us
  blocking collectives: 112 us -> 0 us
  Pallas kernels: 0 us -> 76.8 us
  matrix products: 17 us -> 0 us
  between operations: 13.7 us -> 0.01 us
    all_gather x6 -> x0, waiting for transfers between devices: 799 us -> none  [the longest x4 491 us: taken_in(): lax.all_gather(part, axis, axis=dim, tiled=True)]
    pallas_call x0 -> x1, Pallas kernels: none -> 76.8 us  [fused(): pl.pallas_call(layer_kernel, out_shape=jax.ShapeDtypeStruct((rows, half),...]
    all_gather x3 -> x0, blocking collectives: 73.6 us -> none  [the longest x1 68 us: over_all(): whole = lax.all_gather(shard, axis, axis=dim, tiled=True)]
    psum x1 -> x0, blocking collectives: 38.9 us -> none  [pool_mix(): lax.psum(jnp.sum(floats * floats, axis=-1).astype(jnp.bfloat16), 'tp')]
    reduce_scatter x2 -> x0, waiting for transfers between devices: 33.1 us -> none  [half_step(): lax.psum_scatter(partial_value.astype(jnp.bfloat16), 'tp', scatter_dimens...]
    dot_general x5 -> x0, matrix products: 17 us -> none  [the longest x2 9.93 us: project(): return jnp.dot(hidden, block_cols, preferred_element_type=jnp.float32)]
  transfers between devices with their start and end apart: 8 -> 0, of which waited for: 7 -> 0; matrix products, arithmetic and copies ran while one was open for 1% -> 0% of each run, Pallas kernels for 0% -> 0%
where the time goes in v1:
time: 78.6 us; the launch traced here: 78.4 us
  Pallas kernels  76.8 us (98%)
  local copies, waits for them, and re-layouts  1.67 us (2%)
    pallas_call x1, Pallas kernels, fused(): pl.pallas_call(layer_kernel, out_shape=jax.ShapeDtypeStruct((rows, half),...  76.8 us
    unnamed x1, local copies, waits for them, and re-layouts  1.67 us

profile of v1, /device:TPU:1, one launch (start us, length us, event | category | flops | bytes accessed | tf_op | source)
XLA Modules:
  0.0 78.4 jit_solution(1492058434168509576)
XLA Ops:
  0.0 76.8 %shard_map.118 = bf16[256,512]{1,0:T(8,128)(2,1)} custom-call(bf16[256,512]{1,0:T(8,128)(2,1)} %bitcast.12, f32[1,1024]{1,0:T(1,128)} %bitcast.16, f32[1,512]{1,0:T(1,128)} %bitcast.18, f32[1,512]{1,0:T(1,128)} %bitcast.19, f32[1,1024]{1,0:T(1,128)} %bitcast.17, bf16[16,256]{1,0:T(8,128)(2,1)} %bitcast.15, bf16[32,1280]{1,0:T(8,128)(2,1)} %g1_ref.1, ...), custom_call_target="tpu_custom_call" | custom-call | tf_op jit(solution)/shard_map/pallas_call | solution.py:300
  76.8 1.7 %copy.14 = bf16[1,256,512]{2,1,0:T(8,128)(2,1)} copy(bf16[1,256,512]{2,1,0:T(8,128)(2,1)} %bitcast.11) | data formatting | bytes 524288

commit v2 on v1

--- a/solution.py
+++ b/solution.py
@@ -20,7 +20,7 @@
     tok_ref, pre_ref, mixg_ref, scale_ref, post_ref, pw_ref,
     g1_ref, u1_ref, d1_ref, g2_ref, u2_ref, d2_ref, out_ref,
     WS0, WS1, WB0, WB1, TB, N, ACC, H, PX, PR, PO, S, R, SQ,
-    xs, xr, ys, yr, zs, zr, ts, tr, ms, mr, hs, hr, rs, rr, qs,
+    xs, xr, ys, yr, fw, fr, zs, zr, ts, tr, ms, mr, hs, hr, rs, rr, qs,
 ):
     rep = lax.axis_index("rep")
     fs = lax.axis_index("fs")
@@ -66,15 +66,10 @@
     place = (x, y)
     spot = (y, x)
 
-    def slab(b, lo, a, c):
+    def slab(b, lo, j, c):
+        a = lax.rem(place[b] + j, SIDE)
+        c = lax.rem(spot[b] + c, SIDE)
         return WB[b].at[lo, c, a] if b == 0 else WB[b].at[lo, a, c]
-
-    def line(b, lo, c):
-        return WB[b].at[lo, c] if b == 0 else WB[b].at[lo, :, c]
-
-    def line_half(b, lo, c, k):
-        cut = slice(2 * k, 2 * k + 2)
-        return WB[b].at[lo, c, cut] if b == 0 else WB[b].at[lo, cut, c]
 
     def pack(b):
         for k in range(2):
@@ -85,31 +80,72 @@
                 for i in range(2):
                     WS[b][k, i * 16:(i + 1) * 16, 3 * part:] = flat[:, i * 128:(i + 1) * 128]
         mine = lax.rem(place[b], 2)
-        if b == 0:
-            WB[b][low, y, x] = WS[b][mine]
-        else:
-            WB[b][low, y, x] = WS[b][mine]
-
-    def class_send(b, i):
-        d = (1, 3, 2)[i]
+        WB[b][low, y, x] = WS[b][mine]
+
+    items = [(0, 0), (0, 1), (0, 3), (1, 0), (0, 2)]
+    sides = (0, 0, 1, 1, 0)
+    early = (0,)
+    line_of = {0: 0, 3: 1, 1: 2, 2: 3}
+
+    def class_send(b, j):
+        d = SIDE - j
         kind = lax.rem(place[b] + d, 2)
-        return remote(WS[b].at[kind], slab(b, low, place[b], spot[b]), xs.at[b, i], xr.at[b, i], axis[b][d])
-
-    def ring_send(b, i):
-        c = spot[b]
-        if i < 2:
-            ref = line(b, low, c)
-            return remote(ref, ref, ys.at[b, i], yr.at[b, i], ring[b][(1, 3)[i]])
-        if i == 2:
-            ref = line_half(b, low, lax.rem(c + 3, SIDE), 0)
-            return remote(ref, ref, ys.at[b, i], yr.at[b, i], ring[b][1])
-        ref = line_half(b, low, lax.rem(c + 1, SIDE), 1)
-        return remote(ref, ref, ys.at[b, i], yr.at[b, i], ring[b][3])
-
-    def deep_send(b, j, k):
-        c = lax.rem(spot[b] + (0, 3, 1, 2)[j], SIDE)
-        ref = line_half(b, low, c, k)
-        return remote(ref, ref, zs.at[b, j, k], zr.at[b, j, k], along_z[(1, 3)[k]])
+        return remote(WS[b].at[kind], slab(b, low, 0, 0), xs.at[b, j - 1], xr.at[b, j - 1], axis[b][d])
+
+    def ring_send(b, i, side):
+        comp, j = items[i]
+        ref = slab(b, high if comp else low, j, 0)
+        return remote(ref, ref, ys.at[b, i, side], yr.at[b, i, side], ring[b][(1, 3)[side]])
+
+    def far_send(b, i):
+        comp, j = items[i]
+        side = sides[i] if b == 0 else 1 - sides[i]
+        ref = slab(b, high if comp else low, j, (3, 1)[side])
+        return remote(ref, ref, fw.at[b, i], fr.at[b, i], ring[b][(1, 3)[side]])
+
+    def deep_send(b, j, c):
+        up = j == 1 or (j == 2 and c in (0, 1)) or (j == 0 and b == 0)
+        ref = slab(b, low, j, c)
+        n = line_of[c]
+        return remote(ref, ref, zs.at[b, j, n], zr.at[b, j, n], along_z[1 if up else 3])
+
+    def begin(b):
+        for j in (3, 1, 2):
+            class_send(b, j).start()
+        for side in range(2):
+            ring_send(b, 0, side).start()
+        deep_send(b, 0, 0).start()
+
+    def on_class(b, j):
+        class_send(b, j).wait_recv()
+        for side in range(2):
+            ring_send(b, items.index((0, j)), side).start()
+        deep_send(b, j, 0).start()
+
+    def on_cross(b):
+        deep_send(b, 0, 0).wait_recv()
+        for side in range(2):
+            ring_send(b, items.index((1, 0)), side).start()
+
+    def on_ring(b, i):
+        comp, j = items[i]
+        for side in range(2):
+            ring_send(b, i, side).wait_recv()
+            if side == (sides[i] if b == 0 else 1 - sides[i]):
+                far_send(b, i).start()
+            if not comp and j not in early:
+                deep_send(b, j, (3, 1)[side]).start()
+
+    def on_far(b, i):
+        comp, j = items[i]
+        far_send(b, i).wait_recv()
+        if not comp and j not in early:
+            deep_send(b, j, 2).start()
+
+    def deep_wait(b):
+        for c in (0, 3, 1, 2):
+            for j in (1, 3, 2):
+                deep_send(b, j, c).wait_recv()
 
     def tok_send(b, i):
         src = TB.at[b, t, i * piece:(i + 1) * piece]
@@ -137,14 +173,13 @@
         for c in range(2):
             N[c, cut] = (parts[c] * inv * gain_ref[0:1, c * half:(c + 1) * half]).astype(BF16)
 
-    def gate_up(b, lo, fresh):
+    def gate_up(b, lo, fresh, cut):
         wide = WB[b][lo, :, :, :, 0:2 * part].reshape(half, 2 * part)
-        for cut in chunks:
-            value = jnp.dot(N[lo, cut], wide, preferred_element_type=F32)
-            if fresh:
-                ACC[cut] = value
-            else:
-                ACC[cut] += value
+        value = jnp.dot(N[lo, cut], wide, preferred_element_type=F32)
+        if fresh:
+            ACC[cut] = value
+        else:
+            ACC[cut] += value
 
     def hidden(cut):
         H[cut] = (jax.nn.silu(ACC[cut, 0:part]) * ACC[cut, part:2 * part]).astype(BF16)
@@ -153,8 +188,9 @@
         tall = WB[b][lo, :, :, :, 2 * part:3 * part].reshape(half, part)
         return lax.dot_general(H[cut], tall, NT, preferred_element_type=F32)
 
-    def project(b):
+    def project(b, meanwhile):
         for i, cut in enumerate(chunks):
+            gate_up(b, high, False, cut)
             hidden(cut)
             PX[b, cut] = down(b, cut, other).astype(BF16)
             half_send(b, i).start()
@@ -163,63 +199,57 @@
         S[b] = (PO[chunks[0]] + PR[b, chunks[0]].astype(F32)).astype(BF16)
         for i in range(2):
             back_send(b, i).start()
+        meanwhile()
         half_send(b, 1).wait_recv()
         total = PO[chunks[1]] + PR[b, chunks[1]].astype(F32)
         for i in range(2):
             back_send(b, i).wait_recv()
         return total + R[b].astype(F32)
 
-    def spread(b):
-        for i in range(3):
-            class_send(b, i).wait_recv()
-        for i in range(2):
-            ring_send(b, i).start()
-
-    def relay(b):
-        for k in range(2):
-            deep_send(b, 0, k).start()
-        for i in range(2):
-            ring_send(b, i).wait_recv()
-            ring_send(b, 2 + i).start()
-            for k in range(2):
-                deep_send(b, 1 + i, k).start()
-        for k in range(2):
-            ring_send(b, 2 + k).wait_recv()
-            deep_send(b, 3, k).start()
-
-    def deep_wait(b):
-        for j in range(4):
-            for k in range(2):
-                deep_send(b, j, k).wait_recv()
-
     TB[0, t, 0:rows] = tok_ref[...]
     pack(0)
     pack(1)
     pl.semaphore_wait(barrier, len(peers))
 
-    for i in range(3):
-        class_send(0, i).start()
-    for i in range(3):
-        class_send(1, i).start()
+    begin(0)
     mate_send(0, 2).start()
     for i in range(2):
         tok_send(0, i).start()
+    begin(1)
+    on_class(0, 3)
+    on_class(0, 1)
+    on_cross(0)
     mate_send(0, 2).wait_recv()
     norm_rows(0, chunks[1], pre_ref)
-    spread(0)
+    on_class(0, 2)
     for i in range(2):
         tok_send(0, i).wait_recv()
         mate_send(0, i).start()
-    spread(1)
+    on_ring(0, 0)
+    on_ring(0, 1)
+    on_ring(0, 2)
     for i in range(2):
         mate_send(0, i).wait_recv()
     norm_rows(0, chunks[0], pre_ref)
-    relay(0)
-    gate_up(0, low, True)
-    relay(1)
+    on_class(1, 3)
+    on_class(1, 1)
+    on_ring(0, 3)
+    on_ring(0, 4)
+    on_cross(1)
+    on_class(1, 2)
+    for i in range(5):
+        on_far(0, i)
+    for i in range(5):
+        on_ring(1, i)
+    for cut in chunks:
+        gate_up(0, low, True, cut)
     deep_wait(0)
-    gate_up(0, high, False)
-    first = project(0)
+
+    def fars():
+        for i in range(5):
+            on_far(1, i)
+
+    first = project(0, fars)
 
     after_first = (tok_ref[...].astype(F32) + 0.5 * first).astype(BF16).astype(F32)
     square = after_first * after_first
@@ -264,21 +294,22 @@
     mate_send(1, 2).start()
     mate_send(1, 2).wait_recv()
     norm_rows(1, chunks[1], post_ref)
+    gate_up(1, low, True, chunks[1])
     for i in range(2):
         tok_send(1, i).wait_recv()
         mate_send(1, i).start()
     for i in range(2):
         mate_send(1, i).wait_recv()
     norm_rows(1, chunks[0], post_ref)
-    gate_up(1, low, True)
+    gate_up(1, low, True, chunks[0])
     deep_wait(1)
-    gate_up(1, high, False)
-    second = project(1)
+    second = project(1, lambda: None)
     out_ref[...] = (TB[1, t, 0:rows].astype(F32) + 0.5 * second).astype(BF16)
 
     for b in range(2):
-        sent = [class_send(b, i) for i in range(3)] + [ring_send(b, i) for i in range(4)]
-        sent += [deep_send(b, j, k) for j in range(4) for k in range(2)]
+        sent = [class_send(b, j) for j in (1, 2, 3)] + [far_send(b, i) for i in range(5)]
+        sent += [ring_send(b, i, k) for i in range(5) for k in range(2)]
+        sent += [deep_send(b, j, c) for j in (1, 2, 3) for c in range(SIDE)] + [deep_send(b, 0, 0)]
         sent += [tok_send(b, i) for i in range(2)] + [mate_send(b, i) for i in range(3)]
         sent += [half_send(b, i) for i in range(2)] + [back_send(b, i) for i in range(2)]
         for c in sent:
@@ -317,7 +348,8 @@
             pltpu.VMEM((2, rows, half), BF16),
             pltpu.VMEM((2, rows, half), BF16),
             pltpu.VMEM((2, rows, 128), F32),
-            dma((2, 3)), dma((2, 3)), dma((2, 4)), dma((2, 4)), dma((2, 4, 2)), dma((2, 4, 2)),
+            dma((2, 3)), dma((2, 3)), dma((2, 5, 2)), dma((2, 5, 2)), dma((2, 5)), dma((2, 5)),
+            dma((2, 4, 4)), dma((2, 4, 4)),
             dma((2, 2)), dma((2, 2)), dma((2, 3)), dma((2, 3)), dma((2, 2)), dma((2, 2)),
             dma((2, 2)), dma((2, 2)), dma((2,)),
         ],

time: 78.6 us -> 72.8 us (0.926)
  Pallas kernels: 76.8 us -> 71 us
    pallas_call x1, Pallas kernels: 76.8 us -> 71 us  [fused(): pl.pallas_call(layer_kernel, out_shape=jax.ShapeDtypeStruct((rows, half),...]
where the time goes in v2:
time: 72.8 us; the launch traced here: 72.7 us
  Pallas kernels  71 us (98%)
  local copies, waits for them, and re-layouts  1.67 us (2%)
    pallas_call x1, Pallas kernels, fused(): pl.pallas_call(layer_kernel, out_shape=jax.ShapeDtypeStruct((rows, half),...  71 us
    unnamed x1, local copies, waits for them, and re-layouts  1.67 us

profile of v2, /device:TPU:1, one launch (start us, length us, event | category | flops | bytes accessed | tf_op | source)
XLA Modules:
  0.0 72.7 jit_solution(14342520147299769564)
XLA Ops:
  0.0 71.0 %shard_map.118 = bf16[256,512]{1,0:T(8,128)(2,1)} custom-call(bf16[256,512]{1,0:T(8,128)(2,1)} %bitcast.12, f32[1,1024]{1,0:T(1,128)} %bitcast.16, f32[1,512]{1,0:T(1,128)} %bitcast.18, f32[1,512]{1,0:T(1,128)} %bitcast.19, f32[1,1024]{1,0:T(1,128)} %bitcast.17, bf16[16,256]{1,0:T(8,128)(2,1)} %bitcast.15, bf16[32,1280]{1,0:T(8,128)(2,1)} %g1_ref.1, ...), custom_call_target="tpu_custom_call" | custom-call | tf_op jit(solution)/shard_map/pallas_call | solution.py:331
  71.0 1.7 %copy.14 = bf16[1,256,512]{2,1,0:T(8,128)(2,1)} copy(bf16[1,256,512]{2,1,0:T(8,128)(2,1)} %bitcast.11) | data formatting | bytes 524288

commit v3 on v1

v3 whole, which is shorter than its diff:
```python
import jax
import jax.numpy as jnp
from jax import lax
from jax.experimental import pallas as pl
from jax.experimental.pallas import tpu as pltpu
from jax.sharding import PartitionSpec as P

F32 = jnp.float32
BF16 = jnp.bfloat16
MESH = pl.DeviceIdType.MESH
GROUPS = 4
SIDE = 4
epsilon = 1e-06
NT = (((1,), (1,)), ((), ()))

PLAN = (
    (
        ("c", 1, 1), ("c", 0, 3), ("c", 0, 1), ("c", 1, 3), ("z", 0, 0, 0, 1), ("z", 1, 0, 0, 0), ("c", 1, 2),
        ("z", 3, 0, 0, 0), ("r", 1, 0, 0, 0), ("r", 1, 0, 0, 1), ("z", 2, 0, 0, 1), ("r", 0, 0, 0, 1),
        ("t", 1, 0), ("c", 0, 2), ("z", 1, 1, 0, 0), ("z", 1, 3, 0, 1), ("r", 0, 0, 1, 1), ("r", 1, 0, 3, 0),
        ("r", 1, 0, 1, 1), ("z", 0, 3, 0, 0), ("z", 0, 1, 0, 1), ("r", 0, 0, 1, 0), ("r", 1, 0, 1, 0),
        ("r", 1, 0, 3, 1), ("r", 0, 1, 0, 1), ("z", 1, 2, 0, 0), ("r", 0, 0, 3, 0), ("r", 1, 0, 2, 0),
        ("r", 1, 1, 0, 1), ("r", 0, 0, 3, 1), ("z", 0, 2, 0, 0), ("z", 0, 1, 1, 1), ("f", 1, 0, 1, 1),
        ("f", 1, 0, 3, 0), ("r", 0, 0, 0, 0), ("r", 0, 0, 2, 1),
    ),
    (
        ("z", 1, 1, 3, 0), ("t", 0, 0), ("f", 1, 0, 0, 1), ("z", 0, 1, 3, 1), ("f", 0, 0, 1, 0), ("t", 1, 1),
        ("z", 1, 1, 1, 0), ("r", 1, 0, 2, 1), ("z", 1, 3, 3, 1), ("r", 0, 1, 0, 0), ("z", 0, 3, 3, 0),
        ("t", 0, 1), ("f", 1, 0, 2, 0), ("z", 1, 3, 2, 1), ("f", 0, 0, 3, 1), ("r", 0, 0, 2, 0),
        ("z", 0, 3, 1, 0), ("r", 1, 1, 0, 0), ("z", 1, 2, 3, 1), ("c", 3, 1), ("c", 3, 3), ("r", 0, 1, 2, 0),
        ("r", 0, 1, 2, 1), ("z", 1, 2, 1, 0), ("z", 0, 1, 2, 1), ("c", 3, 2), ("z", 1, 1, 2, 0),
        ("f", 0, 0, 2, 1), ("f", 0, 0, 0, 0), ("z", 1, 2, 2, 1), ("r", 2, 1, 0, 0), ("r", 2, 0, 0, 1),
    ),
    (
        ("z", 0, 3, 2, 0), ("z", 1, 3, 1, 1), ("f", 0, 1, 0, 1), ("c", 2, 3), ("f", 1, 1, 0, 0),
        ("r", 2, 1, 0, 1), ("z", 3, 1, 0, 0), ("z", 3, 3, 0, 1), ("f", 0, 1, 2, 0), ("c", 2, 1),
        ("r", 2, 0, 0, 0), ("z", 3, 2, 0, 0),
    ),
    (
        ("c", 2, 2), ("r", 2, 0, 3, 0), ("r", 2, 0, 3, 1), ("z", 2, 3, 0, 0), ("r", 3, 0, 2, 0),
        ("r", 3, 0, 1, 1), ("r", 2, 0, 1, 1), ("r", 2, 0, 1, 0), ("z", 2, 1, 0, 1), ("r", 3, 0, 1, 0),
        ("r", 3, 0, 3, 1),
    ),
    (
        ("r", 3, 0, 3, 0), ("r", 3, 0, 2, 1), ("f", 2, 1, 0, 1), ("f", 2, 0, 0, 0), ("z", 2, 2, 0, 0),
        ("r", 3, 1, 0, 0), ("r", 3, 1, 0, 1), ("z", 3, 2, 3, 1), ("z", 3, 3, 1, 1), ("z", 2, 3, 1, 0),
        ("z", 3, 3, 3, 1), ("z", 3, 1, 3, 0), ("z", 2, 1, 3, 1), ("f", 2, 0, 3, 1), ("f", 2, 0, 1, 0),
        ("f", 3, 0, 1, 1), ("f", 3, 0, 3, 0), ("z", 3, 1, 1, 0), ("f", 3, 0, 2, 0), ("r", 3, 0, 0, 1),
        ("z", 2, 1, 1, 1), ("r", 2, 0, 2, 1), ("r", 2, 1, 2, 0), ("z", 3, 2, 1, 0),
    ),
    (
        ("r", 3, 0, 0, 0), ("z", 2, 3, 3, 0), ("r", 2, 1, 2, 1), ("r", 2, 0, 2, 0), ("f", 3, 1, 0, 0),
        ("z", 3, 3, 2, 1), ("z", 2, 3, 2, 0), ("f", 3, 0, 0, 1), ("z", 2, 1, 2, 1), ("f", 2, 1, 2, 0),
        ("f", 2, 0, 2, 1), ("z", 3, 1, 2, 0), ("z", 3, 2, 2, 1),
    ),
    (

    ),
)

WAVES = [op for part in PLAN for op in part]
RING_SIDE = {(op[1], op[3]): op[4] for op in WAVES if op[0] == "f" and op[2] == 0}
RISE = {op[1:4]: op[4] for op in WAVES if op[0] == "z"}
COPIES = {op: i for i, op in enumerate(op for op in WAVES if op[0] != "t")}


def sources(op):
    kind, s = op[:2]
    if kind == "c" or kind == "t":
        return []
    if kind == "r":
        _, _, comp, j, _ = op
        if comp:
            return [("z", s, j, 0, RISE[s, j, 0])]
        return [("c", s, j)] if j else []
    if kind == "f":
        return [("r",) + op[1:]]
    _, _, j, c, _ = op
    if c == 0:
        return [("c", s, j)] if j else []
    if c == 2:
        return [("f", s, 0, j, RING_SIDE[s, j])]
    return [("r", s, 0, j, 0 if c == 3 else 1)]


def layer_kernel(
    tok_ref, pre_ref, mixg_ref, scale_ref, post_ref, pw_ref,
    g1_ref, u1_ref, d1_ref, g2_ref, u2_ref, d2_ref, out_ref,
    WS0, WS1, WS2, WS3, WB0, WB1, WB2, WB3, TB, N, ACC0, ACC1, H0, H1, PX, PR, PO, S, R, SQ,
    ws, wr, ts, tr, ms, mr, hs, hr, rs, rr, qs,
):
    rep = lax.axis_index("rep")
    fs = lax.axis_index("fs")
    t = lax.axis_index("tp")
    x = lax.rem(fs, SIDE)
    y = lax.rem(fs // SIDE, SIDE)
    low = fs // (SIDE * SIDE)
    z = 2 * rep + low
    other = 1 - t
    high = 1 - low

    def dev(dx, dy, dz, tt):
        xx = lax.rem(x + dx, SIDE)
        yy = lax.rem(y + dy, SIDE)
        zz = lax.rem(z + dz, SIDE)
        return {"rep": zz // 2, "fs": lax.rem(zz, 2) * (SIDE * SIDE) + yy * SIDE + xx, "tp": tt}

    mate = dev(0, 0, 0, other)
    along_x = {d: dev(d, 0, 0, t) for d in (1, 2, 3)}
    along_y = {d: dev(0, d, 0, t) for d in (1, 2, 3)}
    along_z = {d: dev(0, 0, d, t) for d in (1, 3)}
    peers = [mate] + list(along_x.values()) + list(along_y.values()) + list(along_z.values())

    barrier = pltpu.get_barrier_semaphore()
    for peer in peers:
        pl.semaphore_signal(barrier, inc=1, device_id=peer, device_id_type=MESH)

    def remote(src, dst, ss, sr, to):
        return pltpu.make_async_remote_copy(
            src_ref=src, dst_ref=dst, send_sem=ss, recv_sem=sr, device_id=to, device_id_type=MESH
        )

    rows, half = tok_ref.shape
    depth, hid = g1_ref.shape
    piece = rows // 2
    widths = (H0.shape[1], H1.shape[1])
    weights = ((g1_ref, u1_ref, d1_ref), (g2_ref, u2_ref, d2_ref))
    WS = (WS0, WS1, WS2, WS3)
    WB = (WB0, WB1, WB2, WB3)
    ACC = (ACC0, ACC1)
    H = (H0, H1)
    axes = (along_x, along_y)
    turn = (0, 1, 1, 0)
    places = (x, y)

    def slab(s, lo, j, c):
        a = lax.rem(places[turn[s]] + j, SIDE)
        c = lax.rem(places[1 - turn[s]] + c, SIDE)
        return WB[s].at[lo, c, a] if turn[s] == 0 else WB[s].at[lo, a, c]

    def pack(s):
        b, p = divmod(s, 2)
        n = widths[p]
        start = 2 * widths[0] * p
        for k in range(2):
            for i, w in enumerate(weights[b]):
                WS[s][k, :, i * n:(i + 1) * n] = w[:, start + k * n:start + (k + 1) * n]
            if s == 1:
                flat = pw_ref[...]
                for i in range(2):
                    WS[s][k, i * 16:(i + 1) * 16, 3 * n:] = flat[:, i * 128:(i + 1) * 128]
        WB[s][low, y, x] = WS[s][lax.rem(places[turn[s]], 2)]

    def copy_of(op):
        kind = op[0]
        if kind == "t":
            return tok_send(0, op[1], op[2])
        s = op[1]
        axis, ring = axes[turn[s]], axes[1 - turn[s]]
        sems = (ws.at[COPIES[op]], wr.at[COPIES[op]])
        if kind == "c":
            d = SIDE - op[2]
            src = WS[s].at[lax.rem(places[turn[s]] + d, 2)]
            return remote(src, slab(s, low, 0, 0), *sems, axis[d])
        if kind == "r":
            _, _, comp, j, side = op
            ref = slab(s, high if comp else low, j, 0)
            return remote(ref, ref, *sems, ring[(1, 3)[side]])
        if kind == "f":
            _, _, comp, j, side = op
            ref = slab(s, high if comp else low, j, (3, 1)[side])
            return remote(ref, ref, *sems, ring[(1, 3)[side]])
        _, _, j, c, up = op
        ref = slab(s, low, j, c)
        return remote(ref, ref, *sems, along_z[1 if up else 3])

    here = set()

    def need(op):
        if op not in here:
            here.add(op)
            copy_of(op).wait_recv()

    def issue(part):
        for op in PLAN[part]:
            for source in sources(op):
                need(source)
            copy_of(op).start()

    def base(p):
        return rows * (1 + p)

    own = slice(0, rows)
    foreign = tuple(slice(base(p), base(p) + rows) for p in range(2))

    def axis_of(b, p):
        return axes[turn[2 * b + p]]

    def tok_send(b, p, i):
        src = TB.at[b, t, i * piece:(i + 1) * piece]
        dst = TB.at[b, t, base(p) + i * piece:base(p) + (i + 1) * piece]
        return remote(src, dst, ts.at[b, p, i], tr.at[b, p, i], axis_of(b, p)[(1, 3)[i]])

    def mate_send(b, n):
        cut = own if n == 4 else slice(rows + n * piece, rows + (n + 1) * piece)
        ref = TB.at[b, t, cut]
        return remote(ref, ref, ms.at[b, n], mr.at[b, n], mate)

    def half_send(b, n):
        cut = own if n == 2 else foreign[n]
        return remote(PX.at[b, cut], PR.at[b, cut], hs.at[b, n], hr.at[b, n], mate)

    def back_send(b, p, i):
        cut = slice(i * piece, (i + 1) * piece)
        return remote(
            S.at[b, p, cut], R.at[b, p, cut], rs.at[b, p, i], rr.at[b, p, i], axis_of(b, p)[(3, 1)[i]]
        )

    def norm_rows(b, cut, gain_ref):
        parts = [TB[b, c, cut].astype(F32) for c in range(2)]
        total = sum(jnp.sum(v * v, axis=-1, keepdims=True) for v in parts)
        inv = lax.rsqrt(total / (2 * half) + epsilon)
        for c in range(2):
            N[c, cut] = (parts[c] * inv * gain_ref[0:1, c * half:(c + 1) * half]).astype(BF16)

    def gate_up(b, p, lo, fresh, cut):
        n = 2 * widths[p]
        wide = WB[2 * b + p][lo, :, :, :, 0:n].reshape(half, n)
        value = jnp.dot(N[lo, cut], wide, preferred_element_type=F32)
        at = own if cut is own else slice(rows, 2 * rows)
        if fresh:
            ACC[p][at] = value
        else:
            ACC[p][at] += value

    def hidden(p, cut):
        at = own if cut is own else slice(rows, 2 * rows)
        n = widths[p]
        H[p][at] = (jax.nn.silu(ACC[p][at, 0:n]) * ACC[p][at, n:2 * n]).astype(BF16)

    def down(b, p, cut, lo):
        at = own if cut is own else slice(rows, 2 * rows)
        n = widths[p]
        tall = WB[2 * b + p][lo, :, :, :, 2 * n:3 * n].reshape(half, n)
        return lax.dot_general(H[p][at], tall, NT, preferred_element_type=F32)

    def project(b, last, meanwhile):
        for p in range(2):
            cut = foreign[p]
            gate_up(b, p, last, False, cut)
            hidden(p, cut)
            PX[b, cut] = down(b, p, cut, other).astype(BF16)
            half_send(b, p).start()
            PO[cut] = down(b, p, cut, t)
        for p in range(2):
            gate_up(b, p, last, False, own)
            hidden(p, own)
        PX[b, own] = (down(b, 0, own, other) + down(b, 1, own, other)).astype(BF16)
        half_send(b, 2).start()
        for p in range(2):
            cut = foreign[p]
            half_send(b, p).wait_recv()
            S[b, p] = (PO[cut] + PR[b, cut].astype(F32)).astype(BF16)
            for i in range(2):
                back_send(b, p, i).start()
        PO[own] = down(b, 0, own, t) + down(b, 1, own, t)
        meanwhile()
        half_send(b, 2).wait_recv()
        total = PO[own] + PR[b, own].astype(F32)
        for p in range(2):
            for i in range(2):
                back_send(b, p, i).wait_recv()
            total = total + R[b, p].astype(F32)
        return total

    def all_of(b):
        return [op for op in COPIES if op[1] // 2 == b]

    def first_half(op):
        return op[0] == "c" or (op[0] in "rf" and op[2] == 0)

    TB[0, t, own] = tok_ref[...]
    for s in range(4):
        pack(s)
    pl.semaphore_wait(barrier, len(peers))

    mate_send(0, 4).start()
    issue(0)
    mate_send(0, 4).wait_recv()
    norm_rows(0, own, pre_ref)
    issue(1)
    for p in range(2):
        for i in range(2):
            tok_send(0, p, i).wait_recv()
            mate_send(0, 2 * p + i).start()
    issue(2)
    for p in range(2):
        for i in range(2):
            mate_send(0, 2 * p + i).wait_recv()
        norm_rows(0, foreign[p], pre_ref)
    issue(3)
    for op in all_of(0):
        if first_half(op):
            need(op)
    for p in range(2):
        gate_up(0, p, low, True, foreign[p])
        gate_up(0, p, low, True, own)
    for op in all_of(0):
        need(op)
    first = project(0, high, lambda: issue(4))

    after_first = (tok_ref[...].astype(F32) + 0.5 * first).astype(BF16).astype(F32)
    square = after_first * after_first
    SQ[0] = sum(square[:, i * 128:(i + 1) * 128] for i in range(half // 128))
    swap = remote(SQ.at[0], SQ.at[1], qs.at[0], qs.at[1], mate)
    swap.start()
    swap.wait_recv()
    total = jnp.sum(SQ[0] + SQ[1], axis=-1, keepdims=True)
    h = (after_first * lax.rsqrt(total / (2 * half) + epsilon) * mixg_ref[0:1, :]).astype(BF16).astype(F32)
    groups_here = 2
    width = half // groups_here

    def shifted(v, by):
        spot_ids = lax.broadcasted_iota(jnp.int32, v.shape, 0)
        return jnp.where(spot_ids >= by, pltpu.roll(v, by, 0), 0.0)

    maps = WB1[:, :, :, :, 3 * widths[1]:].reshape(2 * SIDE * SIDE, depth, 128).astype(F32)
    maps = maps.reshape(2 * SIDE * SIDE, 4, 8, 128)
    for g in range(groups_here):
        hg = h[:, g * width:(g + 1) * width]
        run = hg + shifted(hg, 1)
        window = 2
        found = run
        number = t * groups_here + g
        reached = jnp.int32(2)
        for level in range(1, GROUPS):
            run = run + shifted(run, window)
            window = window * 2
            found = jnp.where(number >= level, run, found)
            reached = jnp.where(number >= level, window, reached)
        counts = jnp.minimum(lax.broadcasted_iota(jnp.int32, (rows, width), 0) + 1, reached).astype(F32)
        diff = (found / counts - hg).astype(BF16)
        turned = jnp.concatenate(
            [maps[:, g].reshape(width, 128), maps[:, 2 + g].reshape(width, 128)], axis=1
        ).astype(BF16)
        mixed = lax.dot_general(diff, turned, NT, preferred_element_type=F32)
        at = slice(g * width, (g + 1) * width)
        TB[1, t, own, at] = (after_first[:, at] + scale_ref[0:1, at] * mixed).astype(BF16)

    for p in range(2):
        for i in range(2):
            tok_send(1, p, i).start()
    mate_send(1, 4).start()
    mate_send(1, 4).wait_recv()
    norm_rows(1, own, post_ref)
    issue(5)
    for p in range(2):
        for i in range(2):
            tok_send(1, p, i).wait_recv()
            mate_send(1, 2 * p + i).start()
    issue(6)
    for op in all_of(1):
        if first_half(op):
            need(op)
    for p in range(2):
        gate_up(1, p, low, True, own)
    for p in range(2):
        for i in range(2):
            mate_send(1, 2 * p + i).wait_recv()
        norm_rows(1, foreign[p], post_ref)
        gate_up(1, p, low, True, foreign[p])
    for op in all_of(1):
        need(op)
    second = project(1, high, lambda: None)
    out_ref[...] = (TB[1, t, own].astype(F32) + 0.5 * second).astype(BF16)

    for op in COPIES:
        copy_of(op).wait_send()
    for b in range(2):
        sent = [tok_send(b, p, i) for p in range(2) for i in range(2)]
        sent += [back_send(b, p, i) for p in range(2) for i in range(2)]
        sent += [mate_send(b, n) for n in range(5)] + [half_send(b, n) for n in range(3)]
        for c in sent:
            c.wait_send()
    swap.wait_send()


def fused(
    tokens, pre_gain, first_gate, first_up, first_down, mix_gain, pool_weight,
    pool_scale, post_gain, second_gate, second_up, second_down,
):
    _, rows, half = tokens.shape
    depth, hid = first_gate.shape
    wide = 3 * hid // 10
    slim = hid // 2 - wide
    groups, width, out_cols = pool_weight.shape
    lanes = (3 * wide, 3 * slim + 128, 3 * wide, 3 * slim)

    vmem = pl.BlockSpec(memory_space=pltpu.VMEM)
    dma = pltpu.SemaphoreType.DMA
    out = pl.pallas_call(
        layer_kernel,
        out_shape=jax.ShapeDtypeStruct((rows, half), BF16),
        in_specs=[vmem] * 12,
        out_specs=vmem,
        scratch_shapes=[pltpu.VMEM((2, depth, n), BF16) for n in lanes]
        + [pltpu.VMEM((2, SIDE, SIDE, depth, n), BF16) for n in lanes]
        + [
            pltpu.VMEM((2, 2, 3 * rows, half), BF16),
            pltpu.VMEM((2, 3 * rows, half), BF16),
            pltpu.VMEM((2 * rows, 2 * wide), F32),
            pltpu.VMEM((2 * rows, 2 * slim), F32),
            pltpu.VMEM((2 * rows, wide), BF16),
            pltpu.VMEM((2 * rows, slim), BF16),
            pltpu.VMEM((2, 3 * rows, half), BF16),
            pltpu.VMEM((2, 3 * rows, half), BF16),
            pltpu.VMEM((3 * rows, half), F32),
            pltpu.VMEM((2, 2, rows, half), BF16),
            pltpu.VMEM((2, 2, rows, half), BF16),
            pltpu.VMEM((2, rows, 128), F32),
            dma((len(COPIES),)), dma((len(COPIES),)),
            dma((2, 2, 2)), dma((2, 2, 2)), dma((2, 5)), dma((2, 5)), dma((2, 3)), dma((2, 3)),
            dma((2, 2, 2)), dma((2, 2, 2)), dma((2,)),
        ],
        compiler_params=pltpu.CompilerParams(
            collective_id=0, has_side_effects=True, vmem_limit_bytes=60 * 1024 * 1024
        ),
    )(
        tokens.reshape(rows, half), pre_gain.reshape(1, -1), mix_gain.reshape(1, -1),
        pool_scale.reshape(1, -1), post_gain.reshape(1, -1),
        jnp.swapaxes(pool_weight, 1, 2).reshape(groups * out_cols, width),
        first_gate, first_up, first_down.T, second_gate, second_up, second_down.T,
    )
    return out.reshape(tokens.shape)


def solution(mesh):
    tok = P(("rep", "fs"), None, "tp")
    wide = P("fs", "tp")
    tall = P("tp", "fs")
    placed = (
        tok, P(), wide, wide, tall, P("tp"), P("tp", None, "fs"), P("tp"), P(), wide, wide, tall,
    )

    def layer(*args):
        return jax.shard_map(fused, mesh=mesh, in_specs=placed, out_specs=tok, check_vma=False)(*args)

    return layer
```

time: 78.6 us -> 71.2 us (0.906)
  Pallas kernels: 76.8 us -> 69.4 us
    pallas_call x1, Pallas kernels: 76.8 us -> 69.4 us  [fused(): pl.pallas_call(layer_kernel, out_shape=jax.ShapeDtypeStruct((rows, half),...]
where the time goes in v3:
time: 71.2 us; the launch traced here: 71.1 us
  Pallas kernels  69.4 us (97%)
  local copies, waits for them, and re-layouts  1.67 us (2%)
    pallas_call x1, Pallas kernels, fused(): pl.pallas_call(layer_kernel, out_shape=jax.ShapeDtypeStruct((rows, half),...  69.4 us
    unnamed x1, local copies, waits for them, and re-layouts  1.67 us

profile of v3, /device:TPU:1, one launch (start us, length us, event | category | flops | bytes accessed | tf_op | source)
XLA Modules:
  0.0 71.1 jit_solution(15073937498077051986)
XLA Ops:
  0.0 69.4 %shard_map.118 = bf16[256,512]{1,0:T(8,128)(2,1)} custom-call(bf16[256,512]{1,0:T(8,128)(2,1)} %bitcast.12, f32[1,1024]{1,0:T(1,128)} %bitcast.16, f32[1,512]{1,0:T(1,128)} %bitcast.18, f32[1,512]{1,0:T(1,128)} %bitcast.19, f32[1,1024]{1,0:T(1,128)} %bitcast.17, bf16[16,256]{1,0:T(8,128)(2,1)} %bitcast.15, bf16[32,1280]{1,0:T(8,128)(2,1)} %g1_ref.1, ...), custom_call_target="tpu_custom_call" | custom-call | tf_op jit(solution)/shard_map/pallas_call | solution.py:401
  69.4 1.7 %copy.14 = bf16[1,256,512]{2,1,0:T(8,128)(2,1)} copy(bf16[1,256,512]{2,1,0:T(8,128)(2,1)} %bitcast.11) | data formatting | bytes 524288

commit v4 on v3

--- a/solution.py
+++ b/solution.py
@@ -15,46 +15,52 @@
 
 PLAN = (
     (
-        ("c", 1, 1), ("c", 0, 3), ("c", 0, 1), ("c", 1, 3), ("z", 0, 0, 0, 1), ("z", 1, 0, 0, 0), ("c", 1, 2),
+        ("c", 1, 3), ("c", 0, 1), ("c", 1, 1), ("z", 0, 0, 0, 1), ("c", 0, 3), ("z", 1, 0, 0, 0), ("c", 1, 2),
         ("z", 3, 0, 0, 0), ("r", 1, 0, 0, 0), ("r", 1, 0, 0, 1), ("z", 2, 0, 0, 1), ("r", 0, 0, 0, 1),
-        ("t", 1, 0), ("c", 0, 2), ("z", 1, 1, 0, 0), ("z", 1, 3, 0, 1), ("r", 0, 0, 1, 1), ("r", 1, 0, 3, 0),
-        ("r", 1, 0, 1, 1), ("z", 0, 3, 0, 0), ("z", 0, 1, 0, 1), ("r", 0, 0, 1, 0), ("r", 1, 0, 1, 0),
-        ("r", 1, 0, 3, 1), ("r", 0, 1, 0, 1), ("z", 1, 2, 0, 0), ("r", 0, 0, 3, 0), ("r", 1, 0, 2, 0),
-        ("r", 1, 1, 0, 1), ("r", 0, 0, 3, 1), ("z", 0, 2, 0, 0), ("z", 0, 1, 1, 1), ("f", 1, 0, 1, 1),
-        ("f", 1, 0, 3, 0), ("r", 0, 0, 0, 0), ("r", 0, 0, 2, 1),
-    ),
-    (
-        ("z", 1, 1, 3, 0), ("t", 0, 0), ("f", 1, 0, 0, 1), ("z", 0, 1, 3, 1), ("f", 0, 0, 1, 0), ("t", 1, 1),
-        ("z", 1, 1, 1, 0), ("r", 1, 0, 2, 1), ("z", 1, 3, 3, 1), ("r", 0, 1, 0, 0), ("z", 0, 3, 3, 0),
-        ("t", 0, 1), ("f", 1, 0, 2, 0), ("z", 1, 3, 2, 1), ("f", 0, 0, 3, 1), ("r", 0, 0, 2, 0),
-        ("z", 0, 3, 1, 0), ("r", 1, 1, 0, 0), ("z", 1, 2, 3, 1), ("c", 3, 1), ("c", 3, 3), ("r", 0, 1, 2, 0),
-        ("r", 0, 1, 2, 1), ("z", 1, 2, 1, 0), ("z", 0, 1, 2, 1), ("c", 3, 2), ("z", 1, 1, 2, 0),
-        ("f", 0, 0, 2, 1), ("f", 0, 0, 0, 0), ("z", 1, 2, 2, 1), ("r", 2, 1, 0, 0), ("r", 2, 0, 0, 1),
-    ),
-    (
-        ("z", 0, 3, 2, 0), ("z", 1, 3, 1, 1), ("f", 0, 1, 0, 1), ("c", 2, 3), ("f", 1, 1, 0, 0),
-        ("r", 2, 1, 0, 1), ("z", 3, 1, 0, 0), ("z", 3, 3, 0, 1), ("f", 0, 1, 2, 0), ("c", 2, 1),
-        ("r", 2, 0, 0, 0), ("z", 3, 2, 0, 0),
-    ),
-    (
-        ("c", 2, 2), ("r", 2, 0, 3, 0), ("r", 2, 0, 3, 1), ("z", 2, 3, 0, 0), ("r", 3, 0, 2, 0),
-        ("r", 3, 0, 1, 1), ("r", 2, 0, 1, 1), ("r", 2, 0, 1, 0), ("z", 2, 1, 0, 1), ("r", 3, 0, 1, 0),
-        ("r", 3, 0, 3, 1),
-    ),
-    (
-        ("r", 3, 0, 3, 0), ("r", 3, 0, 2, 1), ("f", 2, 1, 0, 1), ("f", 2, 0, 0, 0), ("z", 2, 2, 0, 0),
-        ("r", 3, 1, 0, 0), ("r", 3, 1, 0, 1), ("z", 3, 2, 3, 1), ("z", 3, 3, 1, 1), ("z", 2, 3, 1, 0),
-        ("z", 3, 3, 3, 1), ("z", 3, 1, 3, 0), ("z", 2, 1, 3, 1), ("f", 2, 0, 3, 1), ("f", 2, 0, 1, 0),
-        ("f", 3, 0, 1, 1), ("f", 3, 0, 3, 0), ("z", 3, 1, 1, 0), ("f", 3, 0, 2, 0), ("r", 3, 0, 0, 1),
-        ("z", 2, 1, 1, 1), ("r", 2, 0, 2, 1), ("r", 2, 1, 2, 0), ("z", 3, 2, 1, 0),
-    ),
-    (
-        ("r", 3, 0, 0, 0), ("z", 2, 3, 3, 0), ("r", 2, 1, 2, 1), ("r", 2, 0, 2, 0), ("f", 3, 1, 0, 0),
-        ("z", 3, 3, 2, 1), ("z", 2, 3, 2, 0), ("f", 3, 0, 0, 1), ("z", 2, 1, 2, 1), ("f", 2, 1, 2, 0),
-        ("f", 2, 0, 2, 1), ("z", 3, 1, 2, 0), ("z", 3, 2, 2, 1),
-    ),
-    (
-
+        ("t", 1, 0), ("c", 0, 2),
+    ),
+    (
+        ("z", 1, 3, 0, 1), ("z", 1, 1, 0, 0), ("r", 1, 0, 3, 1), ("r", 1, 0, 3, 0), ("r", 1, 0, 1, 1),
+        ("t", 0, 0), ("r", 0, 0, 1, 1), ("z", 0, 1, 0, 1), ("z", 0, 3, 0, 0), ("r", 0, 1, 0, 0),
+        ("r", 0, 0, 3, 1), ("r", 0, 0, 1, 0), ("r", 0, 1, 0, 1), ("r", 0, 0, 3, 0), ("t", 1, 1),
+        ("z", 1, 2, 0, 0), ("r", 1, 0, 2, 1), ("f", 1, 0, 0, 1), ("z", 0, 2, 0, 0), ("r", 0, 0, 2, 0),
+        ("z", 1, 3, 1, 1), ("f", 1, 0, 3, 0), ("z", 1, 3, 3, 1), ("r", 1, 1, 0, 0), ("z", 0, 1, 1, 1),
+        ("r", 1, 0, 1, 0), ("r", 1, 0, 2, 0), ("z", 1, 1, 1, 0), ("f", 1, 0, 1, 1), ("r", 1, 1, 0, 1),
+        ("t", 0, 1), ("z", 0, 3, 1, 0), ("f", 0, 0, 3, 1), ("r", 0, 0, 2, 1), ("z", 1, 2, 1, 0),
+        ("f", 0, 0, 1, 0), ("r", 0, 0, 0, 0), ("c", 2, 3),
+    ),
+    (
+        ("r", 0, 1, 2, 1), ("f", 0, 1, 0, 1), ("r", 0, 1, 2, 0), ("z", 1, 3, 2, 1), ("z", 0, 1, 3, 1),
+        ("z", 0, 3, 3, 0), ("f", 1, 1, 0, 0), ("c", 3, 2), ("c", 3, 1), ("r", 2, 1, 0, 0), ("r", 2, 1, 0, 1),
+        ("r", 2, 0, 0, 1), ("z", 1, 1, 3, 0), ("z", 0, 1, 2, 1), ("z", 0, 3, 2, 0), ("z", 1, 1, 2, 0),
+        ("z", 1, 2, 3, 1), ("f", 1, 0, 2, 0), ("c", 3, 3),
+    ),
+    (
+        ("f", 0, 0, 2, 1), ("f", 0, 0, 0, 0), ("c", 2, 2), ("c", 2, 1), ("z", 3, 2, 0, 1), ("z", 2, 3, 0, 0),
+        ("r", 2, 0, 3, 0), ("r", 2, 0, 3, 1), ("r", 2, 0, 0, 0), ("z", 3, 1, 0, 0), ("r", 3, 0, 1, 1),
+    ),
+    (
+        ("f", 0, 1, 2, 0), ("f", 2, 1, 0, 1), ("z", 1, 2, 2, 1), ("z", 3, 3, 0, 1), ("r", 3, 0, 3, 0),
+        ("r", 3, 0, 1, 0), ("r", 3, 0, 3, 1), ("r", 3, 0, 0, 0), ("r", 3, 0, 2, 1), ("r", 3, 1, 0, 0),
+        ("r", 3, 1, 0, 1),
+    ),
+    (
+        ("z", 2, 3, 3, 0), ("f", 2, 0, 3, 1), ("z", 2, 3, 1, 0), ("r", 2, 0, 2, 0), ("z", 2, 2, 0, 1),
+        ("r", 2, 0, 1, 1), ("r", 2, 0, 1, 0), ("z", 2, 1, 0, 1), ("r", 2, 0, 2, 1),
+    ),
+    (
+        ("z", 3, 1, 1, 0), ("f", 3, 0, 3, 0), ("f", 3, 0, 1, 1), ("z", 3, 3, 3, 1),
+    ),
+    (
+        ("z", 3, 1, 3, 0), ("z", 3, 3, 1, 1), ("r", 3, 0, 0, 1), ("r", 3, 1, 2, 1), ("z", 2, 2, 3, 0),
+        ("f", 2, 0, 2, 0), ("f", 3, 1, 0, 0), ("r", 3, 0, 2, 0), ("r", 3, 1, 2, 0), ("z", 2, 1, 1, 1),
+        ("f", 2, 0, 1, 0), ("f", 2, 0, 0, 0),
+    ),
+    (
+        ("z", 3, 1, 2, 0), ("z", 3, 3, 2, 1), ("z", 2, 3, 2, 0), ("z", 2, 1, 3, 1), ("z", 2, 2, 1, 1),
+    ),
+    (
+        ("z", 2, 2, 2, 0), ("f", 3, 0, 0, 1), ("f", 3, 1, 2, 1), ("f", 3, 0, 2, 0), ("z", 2, 1, 2, 1),
     ),
 )
 
@@ -244,7 +250,7 @@
         tall = WB[2 * b + p][lo, :, :, :, 2 * n:3 * n].reshape(half, n)
         return lax.dot_general(H[p][at], tall, NT, preferred_element_type=F32)
 
-    def project(b, last, meanwhile):
+    def project(b, last, gaps):
         for p in range(2):
             cut = foreign[p]
             gate_up(b, p, last, False, cut)
@@ -252,19 +258,21 @@
             PX[b, cut] = down(b, p, cut, other).astype(BF16)
             half_send(b, p).start()
             PO[cut] = down(b, p, cut, t)
-        for p in range(2):
-            gate_up(b, p, last, False, own)
-            hidden(p, own)
-        PX[b, own] = (down(b, 0, own, other) + down(b, 1, own, other)).astype(BF16)
-        half_send(b, 2).start()
+        gaps[0]()
         for p in range(2):
             cut = foreign[p]
             half_send(b, p).wait_recv()
             S[b, p] = (PO[cut] + PR[b, cut].astype(F32)).astype(BF16)
             for i in range(2):
                 back_send(b, p, i).start()
+        for p in range(2):
+            gate_up(b, p, last, False, own)
+            hidden(p, own)
+        PX[b, own] = (down(b, 0, own, other) + down(b, 1, own, other)).astype(BF16)
+        half_send(b, 2).start()
+        gaps[1]()
         PO[own] = down(b, 0, own, t) + down(b, 1, own, t)
-        meanwhile()
+        gaps[2]()
         half_send(b, 2).wait_recv()
         total = PO[own] + PR[b, own].astype(F32)
         for p in range(2):
@@ -284,30 +292,32 @@
         pack(s)
     pl.semaphore_wait(barrier, len(peers))
 
+    issue(0)
     mate_send(0, 4).start()
-    issue(0)
     mate_send(0, 4).wait_recv()
     norm_rows(0, own, pre_ref)
     issue(1)
+    issue(2)
     for p in range(2):
         for i in range(2):
             tok_send(0, p, i).wait_recv()
             mate_send(0, 2 * p + i).start()
-    issue(2)
+    issue(3)
     for p in range(2):
         for i in range(2):
             mate_send(0, 2 * p + i).wait_recv()
         norm_rows(0, foreign[p], pre_ref)
-    issue(3)
+    issue(4)
     for op in all_of(0):
         if first_half(op):
             need(op)
     for p in range(2):
         gate_up(0, p, low, True, foreign[p])
         gate_up(0, p, low, True, own)
+    issue(5)
     for op in all_of(0):
         need(op)
-    first = project(0, high, lambda: issue(4))
+    first = project(0, high, [lambda: issue(6), lambda: issue(7), lambda: issue(8)])
 
     after_first = (tok_ref[...].astype(F32) + 0.5 * first).astype(BF16).astype(F32)
     square = after_first * after_first
@@ -353,12 +363,11 @@
     mate_send(1, 4).start()
     mate_send(1, 4).wait_recv()
     norm_rows(1, own, post_ref)
-    issue(5)
+    issue(9)
     for p in range(2):
         for i in range(2):
             tok_send(1, p, i).wait_recv()
             mate_send(1, 2 * p + i).start()
-    issue(6)
     for op in all_of(1):
         if first_half(op):
             need(op)
@@ -371,7 +380,7 @@
         gate_up(1, p, low, True, foreign[p])
     for op in all_of(1):
         need(op)
-    second = project(1, high, lambda: None)
+    second = project(1, high, [lambda: None] * 3)
     out_ref[...] = (TB[1, t, own].astype(F32) + 0.5 * second).astype(BF16)
 
     for op in COPIES:

time: 71.2 us -> 66.7 us (0.937)
  Pallas kernels: 69.4 us -> 64.9 us
    pallas_call x1, Pallas kernels: 69.4 us -> 64.9 us  [fused(): pl.pallas_call(layer_kernel, out_shape=jax.ShapeDtypeStruct((rows, half),...]
where the time goes in v4:
time: 66.7 us; the launch traced here: 66.6 us
  Pallas kernels  64.9 us (97%)
  local copies, waits for them, and re-layouts  1.67 us (3%)
    pallas_call x1, Pallas kernels, fused(): pl.pallas_call(layer_kernel, out_shape=jax.ShapeDtypeStruct((rows, half),...  64.9 us
    unnamed x1, local copies, waits for them, and re-layouts  1.67 us

profile of v4, /device:TPU:1, one launch (start us, length us, event | category | flops | bytes accessed | tf_op | source)
XLA Modules:
  0.0 66.6 jit_solution(9182562113970329166)
XLA Ops:
  0.0 64.9 %shard_map.118 = bf16[256,512]{1,0:T(8,128)(2,1)} custom-call(bf16[256,512]{1,0:T(8,128)(2,1)} %bitcast.12, f32[1,1024]{1,0:T(1,128)} %bitcast.16, f32[1,512]{1,0:T(1,128)} %bitcast.18, f32[1,512]{1,0:T(1,128)} %bitcast.19, f32[1,1024]{1,0:T(1,128)} %bitcast.17, bf16[16,256]{1,0:T(8,128)(2,1)} %bitcast.15, bf16[32,1280]{1,0:T(8,128)(2,1)} %g1_ref.1, ...), custom_call_target="tpu_custom_call" | custom-call | tf_op jit(solution)/shard_map/pallas_call | solution.py:410
  64.9 1.7 %copy.14 = bf16[1,256,512]{2,1,0:T(8,128)(2,1)} copy(bf16[1,256,512]{2,1,0:T(8,128)(2,1)} %bitcast.11) | data formatting | bytes 524288

commit v5 on v4

--- a/solution.py
+++ b/solution.py
@@ -67,9 +67,6 @@
 WAVES = [op for part in PLAN for op in part]
 RING_SIDE = {(op[1], op[3]): op[4] for op in WAVES if op[0] == "f" and op[2] == 0}
 RISE = {op[1:4]: op[4] for op in WAVES if op[0] == "z"}
-COPIES = {op: i for i, op in enumerate(op for op in WAVES if op[0] != "t")}
-
-
 def sources(op):
     kind, s = op[:2]
     if kind == "c" or kind == "t":
@@ -89,11 +86,27 @@
     return [("r", s, 0, j, 0 if c == 3 else 1)]
 
 
+def own_rows(op):
+    return op[0] == "c" or (op[0] in "rf" and op[2] == 0)
+
+
+COPIES = [op for op in WAVES if op[0] != "t"]
+WANTED = {source for op in COPIES for source in sources(op)}
+
+
+def arrival(op):
+    return op if op in WANTED else ("low" if own_rows(op) else "high", op[1])
+
+
+ARRIVALS = {key: i for i, key in enumerate(dict.fromkeys(arrival(op) for op in COPIES))}
+
+
 def layer_kernel(
-    tok_ref, pre_ref, mixg_ref, scale_ref, post_ref, pw_ref,
-    g1_ref, u1_ref, d1_ref, g2_ref, u2_ref, d2_ref, out_ref,
-    WS0, WS1, WS2, WS3, WB0, WB1, WB2, WB3, TB, N, ACC0, ACC1, H0, H1, PX, PR, PO, S, R, SQ,
-    ws, wr, ts, tr, ms, mr, hs, hr, rs, rr, qs,
+    tok_hbm, pre_hbm, mixg_hbm, scale_hbm, post_hbm, pw_hbm,
+    g1_hbm, u1_hbm, d1_hbm, g2_hbm, u2_hbm, d2_hbm, out_ref,
+    wide_gain, slim_gain, pw_ref, own_w,
+    WS0, WS1, WS2, WS3, WB0, WB1, WB2, WB3, TB, N, ACC0, ACC1, H0, H1, PX, PR, PO, S, R, SQ, TM, RC,
+    ls, ws, wr, ts, tr, ms, mr, hs, hr, rs, rr, qs,
 ):
     rep = lax.axis_index("rep")
     fs = lax.axis_index("fs")
@@ -121,16 +134,31 @@
     for peer in peers:
         pl.semaphore_signal(barrier, inc=1, device_id=peer, device_id_type=MESH)
 
+    rows, half = out_ref.shape
     def remote(src, dst, ss, sr, to):
         return pltpu.make_async_remote_copy(
             src_ref=src, dst_ref=dst, send_sem=ss, recv_sem=sr, device_id=to, device_id_type=MESH
         )
 
-    rows, half = tok_ref.shape
-    depth, hid = g1_ref.shape
+    depth, hid = g1_hbm.shape
+    loads = [
+        pltpu.make_async_copy(src, dst, ls.at[i])
+        for i, src, dst in (
+            (0, g1_hbm, own_w.at[0, 0]), (0, u1_hbm, own_w.at[0, 1]), (0, d1_hbm, own_w.at[0, 2]),
+            (1, pw_hbm, pw_ref), (2, tok_hbm, TB.at[0, t, 0:rows]),
+            (3, g2_hbm, own_w.at[1, 0]), (3, u2_hbm, own_w.at[1, 1]), (3, d2_hbm, own_w.at[1, 2]),
+            (4, pre_hbm, wide_gain.at[0:1]), (4, post_hbm, wide_gain.at[1:2]),
+            (5, mixg_hbm, slim_gain.at[0:1]), (5, scale_hbm, slim_gain.at[1:2]),
+        )
+    ]
+    for load in loads:
+        load.start()
+
+    def loaded(i, ref):
+        pltpu.make_async_copy(ref, ref, ls.at[i]).wait()
+
     piece = rows // 2
     widths = (H0.shape[1], H1.shape[1])
-    weights = ((g1_ref, u1_ref, d1_ref), (g2_ref, u2_ref, d2_ref))
     WS = (WS0, WS1, WS2, WS3)
     WB = (WB0, WB1, WB2, WB3)
     ACC = (ACC0, ACC1)
@@ -142,20 +170,26 @@
     def slab(s, lo, j, c):
         a = lax.rem(places[turn[s]] + j, SIDE)
         c = lax.rem(places[1 - turn[s]] + c, SIDE)
-        return WB[s].at[lo, c, a] if turn[s] == 0 else WB[s].at[lo, a, c]
+        yy, xx = (c, a) if turn[s] == 0 else (a, c)
+        start = ((lo * SIDE + yy) * SIDE + xx) * depth
+        return WB[s].at[pl.ds(pl.multiple_of(start, depth), depth)]
+
+    def side_of(s, lo, lanes):
+        return WB[s][pl.ds(pl.multiple_of(lo * half, half), half), lanes]
 
     def pack(s):
         b, p = divmod(s, 2)
         n = widths[p]
         start = 2 * widths[0] * p
         for k in range(2):
-            for i, w in enumerate(weights[b]):
-                WS[s][k, :, i * n:(i + 1) * n] = w[:, start + k * n:start + (k + 1) * n]
+            for i in range(3):
+                WS[s][k, :, i * n:(i + 1) * n] = own_w[b, i, :, start + k * n:start + (k + 1) * n]
             if s == 1:
                 flat = pw_ref[...]
                 for i in range(2):
                     WS[s][k, i * 16:(i + 1) * 16, 3 * n:] = flat[:, i * 128:(i + 1) * 128]
-        WB[s][low, y, x] = WS[s][lax.rem(places[turn[s]], 2)]
+        start = ((low * SIDE + y) * SIDE + x) * depth
+        WB[s][pl.ds(pl.multiple_of(start, depth), depth)] = WS[s][lax.rem(places[turn[s]], 2)]
 
     def copy_of(op):
         kind = op[0]
@@ -163,7 +197,7 @@
             return tok_send(0, op[1], op[2])
         s = op[1]
         axis, ring = axes[turn[s]], axes[1 - turn[s]]
-        sems = (ws.at[COPIES[op]], wr.at[COPIES[op]])
+        sems = (ws.at[s], wr.at[ARRIVALS[arrival(op)]])
         if kind == "c":
             d = SIDE - op[2]
             src = WS[s].at[lax.rem(places[turn[s]] + d, 2)]
@@ -205,33 +239,37 @@
     def tok_send(b, p, i):
         src = TB.at[b, t, i * piece:(i + 1) * piece]
         dst = TB.at[b, t, base(p) + i * piece:base(p) + (i + 1) * piece]
-        return remote(src, dst, ts.at[b, p, i], tr.at[b, p, i], axis_of(b, p)[(1, 3)[i]])
+        return remote(src, dst, ts.at[b], tr.at[b, p], axis_of(b, p)[(1, 3)[i]])
+
+    def tok_here(b, p):
+        ref = TB.at[b, t, foreign[p]]
+        remote(ref, ref, ts.at[b], tr.at[b, p], mate).wait_recv()
 
     def mate_send(b, n):
-        cut = own if n == 4 else slice(rows + n * piece, rows + (n + 1) * piece)
-        ref = TB.at[b, t, cut]
-        return remote(ref, ref, ms.at[b, n], mr.at[b, n], mate)
+        ref = TB.at[b, t, own if n == 2 else foreign[n]]
+        return remote(ref, ref, ms.at[b], mr.at[b, n], mate)
 
     def half_send(b, n):
         cut = own if n == 2 else foreign[n]
-        return remote(PX.at[b, cut], PR.at[b, cut], hs.at[b, n], hr.at[b, n], mate)
+        return remote(PX.at[b, cut], PR.at[b, cut], hs.at[b], hr.at[b, n], mate)
 
     def back_send(b, p, i):
         cut = slice(i * piece, (i + 1) * piece)
-        return remote(
-            S.at[b, p, cut], R.at[b, p, cut], rs.at[b, p, i], rr.at[b, p, i], axis_of(b, p)[(3, 1)[i]]
-        )
-
-    def norm_rows(b, cut, gain_ref):
+        return remote(S.at[b, p, cut], R.at[b, p, cut], rs.at[b], rr.at[b, p], axis_of(b, p)[(3, 1)[i]])
+
+    def back_here(b, p):
+        remote(S.at[b, p], R.at[b, p], rs.at[b], rr.at[b, p], mate).wait_recv()
+
+    def norm_rows(b, cut):
         parts = [TB[b, c, cut].astype(F32) for c in range(2)]
         total = sum(jnp.sum(v * v, axis=-1, keepdims=True) for v in parts)
         inv = lax.rsqrt(total / (2 * half) + epsilon)
         for c in range(2):
-            N[c, cut] = (parts[c] * inv * gain_ref[0:1, c * half:(c + 1) * half]).astype(BF16)
+            N[c, cut] = (parts[c] * inv * wide_gain[b:b + 1, c * half:(c + 1) * half]).astype(BF16)
 
     def gate_up(b, p, lo, fresh, cut):
         n = 2 * widths[p]
-        wide = WB[2 * b + p][lo, :, :, :, 0:n].reshape(half, n)
+        wide = side_of(2 * b + p, lo, slice(0, n))
         value = jnp.dot(N[lo, cut], wide, preferred_element_type=F32)
         at = own if cut is own else slice(rows, 2 * rows)
         if fresh:
@@ -247,7 +285,7 @@
     def down(b, p, cut, lo):
         at = own if cut is own else slice(rows, 2 * rows)
         n = widths[p]
-        tall = WB[2 * b + p][lo, :, :, :, 2 * n:3 * n].reshape(half, n)
+        tall = side_of(2 * b + p, lo, slice(2 * n, 3 * n))
         return lax.dot_general(H[p][at], tall, NT, preferred_element_type=F32)
 
     def project(b, last, gaps):
@@ -257,7 +295,8 @@
             hidden(p, cut)
             PX[b, cut] = down(b, p, cut, other).astype(BF16)
             half_send(b, p).start()
-            PO[cut] = down(b, p, cut, t)
+        for p in range(2):
+            PO[foreign[p]] = down(b, p, foreign[p], t)
         gaps[0]()
         for p in range(2):
             cut = foreign[p]
@@ -276,121 +315,132 @@
         half_send(b, 2).wait_recv()
         total = PO[own] + PR[b, own].astype(F32)
         for p in range(2):
-            for i in range(2):
-                back_send(b, p, i).wait_recv()
+            back_here(b, p)
             total = total + R[b, p].astype(F32)
         return total
 
-    def all_of(b):
-        return [op for op in COPIES if op[1] // 2 == b]
-
-    def first_half(op):
-        return op[0] == "c" or (op[0] in "rf" and op[2] == 0)
-
-    TB[0, t, own] = tok_ref[...]
-    for s in range(4):
-        pack(s)
+    groups_here = 2
+    width = half // groups_here
+
+    def ready_pool():
+        issue(8)
+        maps = WB1[:, 3 * widths[1]:].reshape(2 * SIDE * SIDE, depth, 128).astype(F32)
+        maps = maps.reshape(2 * SIDE * SIDE, 4, 8, 128)
+        for g in range(groups_here):
+            TM[g] = jnp.concatenate(
+                [maps[:, g].reshape(width, 128), maps[:, 2 + g].reshape(width, 128)], axis=1
+            ).astype(BF16)
+            reached = 2 * 2 ** g * jnp.where(t == 0, 1, 2 ** groups_here)
+            ages = lax.broadcasted_iota(jnp.int32, (rows, 128), 0) + 1
+            RC[g] = 1.0 / jnp.minimum(ages, reached).astype(F32)
+
+    def slabs(s, n):
+        ref = WB[s].at[0:n * depth]
+        return lambda key: remote(ref, ref, ws.at[s], wr.at[ARRIVALS[key]], mate)
+
+    def need_all(b, mine):
+        for op in COPIES:
+            if op[1] // 2 == b and own_rows(op) == mine and op in WANTED:
+                need(op)
+        for s in (2 * b, 2 * b + 1):
+            key = ("low" if mine else "high", s)
+            n = sum(arrival(op) == key for op in COPIES)
+            if n:
+                slabs(s, n)(key).wait_recv()
+
+    loaded(0, own_w.at[0])
+    loaded(1, pw_ref)
+    pack(0)
+    pack(1)
+    loaded(3, own_w.at[1])
+    pack(2)
+    pack(3)
+    loaded(2, TB.at[0, t, own])
+    loaded(4, wide_gain)
+    loaded(5, slim_gain)
     pl.semaphore_wait(barrier, len(peers))
 
     issue(0)
-    mate_send(0, 4).start()
-    mate_send(0, 4).wait_recv()
-    norm_rows(0, own, pre_ref)
+    mate_send(0, 2).start()
+    mate_send(0, 2).wait_recv()
+    norm_rows(0, own)
     issue(1)
     issue(2)
     for p in range(2):
-        for i in range(2):
-            tok_send(0, p, i).wait_recv()
-            mate_send(0, 2 * p + i).start()
+        tok_here(0, p)
+        mate_send(0, p).start()
     issue(3)
     for p in range(2):
-        for i in range(2):
-            mate_send(0, 2 * p + i).wait_recv()
-        norm_rows(0, foreign[p], pre_ref)
+        mate_send(0, p).wait_recv()
+        norm_rows(0, foreign[p])
     issue(4)
-    for op in all_of(0):
-        if first_half(op):
-            need(op)
+    need_all(0, True)
     for p in range(2):
         gate_up(0, p, low, True, foreign[p])
         gate_up(0, p, low, True, own)
     issue(5)
-    for op in all_of(0):
-        need(op)
-    first = project(0, high, [lambda: issue(6), lambda: issue(7), lambda: issue(8)])
-
-    after_first = (tok_ref[...].astype(F32) + 0.5 * first).astype(BF16).astype(F32)
+    need_all(0, False)
+    first = project(0, high, [lambda: issue(6), lambda: issue(7), ready_pool])
+
+    after_first = (TB[0, t, own].astype(F32) + 0.5 * first).astype(BF16).astype(F32)
     square = after_first * after_first
     SQ[0] = sum(square[:, i * 128:(i + 1) * 128] for i in range(half // 128))
     swap = remote(SQ.at[0], SQ.at[1], qs.at[0], qs.at[1], mate)
     swap.start()
     swap.wait_recv()
     total = jnp.sum(SQ[0] + SQ[1], axis=-1, keepdims=True)
-    h = (after_first * lax.rsqrt(total / (2 * half) + epsilon) * mixg_ref[0:1, :]).astype(BF16).astype(F32)
-    groups_here = 2
-    width = half // groups_here
+    h = (after_first * lax.rsqrt(total / (2 * half) + epsilon) * slim_gain[0:1, :]).astype(BF16).astype(F32)
 
     def shifted(v, by):
         spot_ids = lax.broadcasted_iota(jnp.int32, v.shape, 0)
         return jnp.where(spot_ids >= by, pltpu.roll(v, by, 0), 0.0)
 
-    maps = WB1[:, :, :, :, 3 * widths[1]:].reshape(2 * SIDE * SIDE, depth, 128).astype(F32)
-    maps = maps.reshape(2 * SIDE * SIDE, 4, 8, 128)
     for g in range(groups_here):
         hg = h[:, g * width:(g + 1) * width]
         run = hg + shifted(hg, 1)
         window = 2
         found = run
         number = t * groups_here + g
-        reached = jnp.int32(2)
         for level in range(1, GROUPS):
             run = run + shifted(run, window)
             window = window * 2
             found = jnp.where(number >= level, run, found)
-            reached = jnp.where(number >= level, window, reached)
-        counts = jnp.minimum(lax.broadcasted_iota(jnp.int32, (rows, width), 0) + 1, reached).astype(F32)
-        diff = (found / counts - hg).astype(BF16)
-        turned = jnp.concatenate(
-            [maps[:, g].reshape(width, 128), maps[:, 2 + g].reshape(width, 128)], axis=1
-        ).astype(BF16)
-        mixed = lax.dot_general(diff, turned, NT, preferred_element_type=F32)
+        share = jnp.concatenate([RC[g]] * (width // 128), axis=1)
+        diff = (found * share - hg).astype(BF16)
+        mixed = lax.dot_general(diff, TM[g], NT, preferred_element_type=F32)
         at = slice(g * width, (g + 1) * width)
-        TB[1, t, own, at] = (after_first[:, at] + scale_ref[0:1, at] * mixed).astype(BF16)
+        TB[1, t, own, at] = (after_first[:, at] + slim_gain[1:2, at] * mixed).astype(BF16)
 
     for p in range(2):
         for i in range(2):
             tok_send(1, p, i).start()
-    mate_send(1, 4).start()
-    mate_send(1, 4).wait_recv()
-    norm_rows(1, own, post_ref)
+    mate_send(1, 2).start()
+    mate_send(1, 2).wait_recv()
+    norm_rows(1, own)
     issue(9)
     for p in range(2):
-        for i in range(2):
-            tok_send(1, p, i).wait_recv()
-            mate_send(1, 2 * p + i).start()
-    for op in all_of(1):
-        if first_half(op):
-            need(op)
+        tok_here(1, p)
+        mate_send(1, p).start()
+    need_all(1, True)
     for p in range(2):
         gate_up(1, p, low, True, own)
     for p in range(2):
-        for i in range(2):
-            mate_send(1, 2 * p + i).wait_recv()
-        norm_rows(1, foreign[p], post_ref)
+        mate_send(1, p).wait_recv()
+        norm_rows(1, foreign[p])
         gate_up(1, p, low, True, foreign[p])
-    for op in all_of(1):
-        need(op)
+    need_all(1, False)
     second = project(1, high, [lambda: None] * 3)
     out_ref[...] = (TB[1, t, own].astype(F32) + 0.5 * second).astype(BF16)
 
-    for op in COPIES:
-        copy_of(op).wait_send()
+    for s in range(4):
+        n = sum(op[1] == s for op in COPIES)
+        ref = WB[s].at[0:n * depth]
+        remote(ref, ref, ws.at[s], wr.at[0], mate).wait_send()
     for b in range(2):
-        sent = [tok_send(b, p, i) for p in range(2) for i in range(2)]
-        sent += [back_send(b, p, i) for p in range(2) for i in range(2)]
-        sent += [mate_send(b, n) for n in range(5)] + [half_send(b, n) for n in range(3)]
-        for c in sent:
-            c.wait_send()
+        remote(S.at[b], R.at[b], ts.at[b], tr.at[b, 0], mate).wait_send()
+        remote(S.at[b], R.at[b], rs.at[b], rr.at[b, 0], mate).wait_send()
+        remote(PX.at[b], PR.at[b], ms.at[b], mr.at[b, 0], mate).wait_send()
+        remote(PX.at[b], PR.at[b], hs.at[b], hr.at[b, 0], mate).wait_send()
     swap.wait_send()
 
 
@@ -406,14 +456,21 @@
     lanes = (3 * wide, 3 * slim + 128, 3 * wide, 3 * slim)
 
     vmem = pl.BlockSpec(memory_space=pltpu.VMEM)
+    anyw = pl.BlockSpec(memory_space=pl.ANY)
     dma = pltpu.SemaphoreType.DMA
     out = pl.pallas_call(
         layer_kernel,
         out_shape=jax.ShapeDtypeStruct((rows, half), BF16),
-        in_specs=[vmem] * 12,
+        in_specs=[anyw] * 12,
         out_specs=vmem,
-        scratch_shapes=[pltpu.VMEM((2, depth, n), BF16) for n in lanes]
-        + [pltpu.VMEM((2, SIDE, SIDE, depth, n), BF16) for n in lanes]
+        scratch_shapes=[
+            pltpu.VMEM((2, 2 * half), F32),
+            pltpu.VMEM((2, half), F32),
+            pltpu.VMEM((groups * out_cols, width), BF16),
+            pltpu.VMEM((2, 3, depth, hid), BF16),
+        ]
+        + [pltpu.VMEM((2, depth, n), BF16) for n in lanes]
+        + [pltpu.VMEM((2 * half, n), BF16) for n in lanes]
         + [
             pltpu.VMEM((2, 2, 3 * rows, half), BF16),
             pltpu.VMEM((2, 3 * rows, half), BF16),
@@ -427,9 +484,11 @@
             pltpu.VMEM((2, 2, rows, half), BF16),
             pltpu.VMEM((2, 2, rows, half), BF16),
             pltpu.VMEM((2, rows, 128), F32),
-            dma((len(COPIES),)), dma((len(COPIES),)),
-            dma((2, 2, 2)), dma((2, 2, 2)), dma((2, 5)), dma((2, 5)), dma((2, 3)), dma((2, 3)),
-            dma((2, 2, 2)), dma((2, 2, 2)), dma((2,)),
+            pltpu.VMEM((groups, width, width), BF16),
+            pltpu.VMEM((groups, rows, 128), F32),
+            dma((6,)), dma((4,)), dma((len(ARRIVALS),)),
+            dma((2,)), dma((2, 2)), dma((2,)), dma((2, 3)), dma((2,)), dma((2, 3)),
+            dma((2,)), dma((2, 2)), dma((2,)),
         ],
         compiler_params=pltpu.CompilerParams(
             collective_id=0, has_side_effects=True, vmem_limit_bytes=60 * 1024 * 1024

time: 66.7 us -> 63.5 us (0.952)
  Pallas kernels: 64.9 us -> 61.7 us
    pallas_call x1, Pallas kernels: 64.9 us -> 61.7 us  [fused(): pl.pallas_call(layer_kernel, out_shape=jax.ShapeDtypeStruct((rows, half),...]
where the time goes in v5:
time: 63.5 us; the launch traced here: 63.4 us
  Pallas kernels  61.7 us (97%)
  local copies, waits for them, and re-layouts  1.67 us (3%)
    pallas_call x1, Pallas kernels, fused(): pl.pallas_call(layer_kernel, out_shape=jax.ShapeDtypeStruct((rows, half),...  61.7 us
    unnamed x1, local copies, waits for them, and re-layouts  1.67 us

profile of v5, /device:TPU:1, one launch (start us, length us, event | category | flops | bytes accessed | tf_op | source)
XLA Modules:
  0.0 63.4 jit_solution(14960353203257726525)
XLA Ops:
  0.0 61.7 %shard_map.118 = bf16[256,512]{1,0:T(8,128)(2,1)} custom-call(bf16[256,512]{1,0:T(8,128)(2,1)} %bitcast.12, f32[1,1024]{1,0:T(1,128)} %bitcast.16, f32[1,512]{1,0:T(1,128)} %bitcast.18, f32[1,512]{1,0:T(1,128)} %bitcast.19, f32[1,1024]{1,0:T(1,128)} %bitcast.17, bf16[16,256]{1,0:T(8,128)(2,1)} %bitcast.15, bf16[32,1280]{1,0:T(8,128)(2,1)} %g1_hbm.1, ...), custom_call_target="tpu_custom_call" | custom-call | tf_op jit(solution)/shard_map/pallas_call | solution.py:461
  61.7 1.7 %copy.14 = bf16[1,256,512]{2,1,0:T(8,128)(2,1)} copy(bf16[1,256,512]{2,1,0:T(8,128)(2,1)} %bitcast.11) | data formatting | bytes 524288

commit v6 on v5

--- a/solution.py
+++ b/solution.py
@@ -15,55 +15,58 @@
 
 PLAN = (
     (
-        ("c", 1, 3), ("c", 0, 1), ("c", 1, 1), ("z", 0, 0, 0, 1), ("c", 0, 3), ("z", 1, 0, 0, 0), ("c", 1, 2),
-        ("z", 3, 0, 0, 0), ("r", 1, 0, 0, 0), ("r", 1, 0, 0, 1), ("z", 2, 0, 0, 1), ("r", 0, 0, 0, 1),
-        ("t", 1, 0), ("c", 0, 2),
-    ),
-    (
-        ("z", 1, 3, 0, 1), ("z", 1, 1, 0, 0), ("r", 1, 0, 3, 1), ("r", 1, 0, 3, 0), ("r", 1, 0, 1, 1),
-        ("t", 0, 0), ("r", 0, 0, 1, 1), ("z", 0, 1, 0, 1), ("z", 0, 3, 0, 0), ("r", 0, 1, 0, 0),
-        ("r", 0, 0, 3, 1), ("r", 0, 0, 1, 0), ("r", 0, 1, 0, 1), ("r", 0, 0, 3, 0), ("t", 1, 1),
-        ("z", 1, 2, 0, 0), ("r", 1, 0, 2, 1), ("f", 1, 0, 0, 1), ("z", 0, 2, 0, 0), ("r", 0, 0, 2, 0),
-        ("z", 1, 3, 1, 1), ("f", 1, 0, 3, 0), ("z", 1, 3, 3, 1), ("r", 1, 1, 0, 0), ("z", 0, 1, 1, 1),
-        ("r", 1, 0, 1, 0), ("r", 1, 0, 2, 0), ("z", 1, 1, 1, 0), ("f", 1, 0, 1, 1), ("r", 1, 1, 0, 1),
-        ("t", 0, 1), ("z", 0, 3, 1, 0), ("f", 0, 0, 3, 1), ("r", 0, 0, 2, 1), ("z", 1, 2, 1, 0),
+        ("c", 0, 1), ("c", 1, 3), ("c", 1, 1), ("c", 0, 3), ("z", 0, 0, 0, 1), ("z", 1, 0, 0, 0), ("c", 1, 2),
+        ("z", 3, 0, 0, 0), ("c", 0, 2), ("z", 2, 0, 0, 1), ("r", 0, 0, 0, 1), ("t", 1, 0), ("r", 1, 0, 0, 0),
+        ("r", 1, 0, 0, 1),
+    ),
+    (
+        ("z", 1, 3, 0, 1), ("z", 1, 1, 0, 0), ("r", 1, 0, 3, 0), ("r", 1, 0, 3, 1), ("r", 1, 0, 1, 0),
+        ("r", 0, 0, 3, 1), ("z", 0, 3, 0, 0), ("z", 0, 1, 0, 1), ("r", 0, 0, 1, 0), ("r", 0, 0, 1, 1),
+        ("r", 1, 0, 2, 1), ("z", 1, 2, 0, 0), ("r", 1, 0, 1, 1), ("r", 1, 0, 2, 0), ("r", 1, 1, 0, 0),
+        ("r", 1, 1, 0, 1), ("z", 0, 2, 0, 1), ("r", 0, 0, 2, 0), ("r", 0, 0, 2, 1), ("r", 0, 0, 3, 0),
+        ("r", 0, 1, 0, 0), ("f", 1, 0, 0, 1), ("z", 0, 3, 1, 0), ("z", 1, 3, 3, 1), ("f", 0, 0, 3, 1),
+        ("z", 1, 3, 1, 1), ("f", 1, 0, 3, 0), ("r", 0, 1, 0, 1), ("t", 1, 1), ("z", 1, 1, 3, 0),
+        ("z", 1, 2, 3, 1), ("f", 1, 0, 2, 0), ("f", 1, 0, 1, 1), ("z", 1, 1, 1, 0), ("z", 0, 1, 1, 1),
+        ("t", 0, 1), ("c", 3, 1), ("r", 2, 0, 0, 1), ("r", 2, 1, 0, 1), ("f", 0, 0, 2, 0), ("z", 0, 2, 3, 0),
         ("f", 0, 0, 1, 0), ("r", 0, 0, 0, 0), ("c", 2, 3),
     ),
     (
-        ("r", 0, 1, 2, 1), ("f", 0, 1, 0, 1), ("r", 0, 1, 2, 0), ("z", 1, 3, 2, 1), ("z", 0, 1, 3, 1),
-        ("z", 0, 3, 3, 0), ("f", 1, 1, 0, 0), ("c", 3, 2), ("c", 3, 1), ("r", 2, 1, 0, 0), ("r", 2, 1, 0, 1),
-        ("r", 2, 0, 0, 1), ("z", 1, 1, 3, 0), ("z", 0, 1, 2, 1), ("z", 0, 3, 2, 0), ("z", 1, 1, 2, 0),
-        ("z", 1, 2, 3, 1), ("f", 1, 0, 2, 0), ("c", 3, 3),
-    ),
-    (
-        ("f", 0, 0, 2, 1), ("f", 0, 0, 0, 0), ("c", 2, 2), ("c", 2, 1), ("z", 3, 2, 0, 1), ("z", 2, 3, 0, 0),
-        ("r", 2, 0, 3, 0), ("r", 2, 0, 3, 1), ("r", 2, 0, 0, 0), ("z", 3, 1, 0, 0), ("r", 3, 0, 1, 1),
-    ),
-    (
-        ("f", 0, 1, 2, 0), ("f", 2, 1, 0, 1), ("z", 1, 2, 2, 1), ("z", 3, 3, 0, 1), ("r", 3, 0, 3, 0),
-        ("r", 3, 0, 1, 0), ("r", 3, 0, 3, 1), ("r", 3, 0, 0, 0), ("r", 3, 0, 2, 1), ("r", 3, 1, 0, 0),
-        ("r", 3, 1, 0, 1),
-    ),
-    (
-        ("z", 2, 3, 3, 0), ("f", 2, 0, 3, 1), ("z", 2, 3, 1, 0), ("r", 2, 0, 2, 0), ("z", 2, 2, 0, 1),
-        ("r", 2, 0, 1, 1), ("r", 2, 0, 1, 0), ("z", 2, 1, 0, 1), ("r", 2, 0, 2, 1),
-    ),
-    (
-        ("z", 3, 1, 1, 0), ("f", 3, 0, 3, 0), ("f", 3, 0, 1, 1), ("z", 3, 3, 3, 1),
-    ),
-    (
-        ("z", 3, 1, 3, 0), ("z", 3, 3, 1, 1), ("r", 3, 0, 0, 1), ("r", 3, 1, 2, 1), ("z", 2, 2, 3, 0),
-        ("f", 2, 0, 2, 0), ("f", 3, 1, 0, 0), ("r", 3, 0, 2, 0), ("r", 3, 1, 2, 0), ("z", 2, 1, 1, 1),
-        ("f", 2, 0, 1, 0), ("f", 2, 0, 0, 0),
-    ),
-    (
-        ("z", 3, 1, 2, 0), ("z", 3, 3, 2, 1), ("z", 2, 3, 2, 0), ("z", 2, 1, 3, 1), ("z", 2, 2, 1, 1),
-    ),
-    (
-        ("z", 2, 2, 2, 0), ("f", 3, 0, 0, 1), ("f", 3, 1, 2, 1), ("f", 3, 0, 2, 0), ("z", 2, 1, 2, 1),
+        ("f", 1, 1, 0, 0), ("t", 0, 0), ("c", 3, 3), ("r", 2, 0, 0, 0), ("r", 2, 1, 0, 0), ("c", 3, 2),
+        ("z", 0, 3, 3, 0), ("z", 1, 3, 2, 1), ("z", 0, 2, 1, 1), ("z", 1, 1, 2, 0), ("z", 1, 2, 2, 1),
+        ("z", 0, 3, 2, 0), ("z", 1, 2, 1, 0), ("f", 0, 1, 0, 1), ("c", 2, 1), ("c", 2, 2), ("z", 0, 2, 2, 0),
+        ("z", 0, 1, 2, 1), ("z", 0, 1, 3, 1), ("z", 3, 1, 0, 0),
+    ),
+    (
+        ("f", 0, 0, 0, 0), ("r", 3, 0, 3, 1), ("r", 3, 0, 1, 1), ("r", 3, 0, 3, 0), ("r", 3, 1, 0, 1),
+        ("r", 3, 0, 1, 0), ("r", 3, 0, 0, 1), ("r", 3, 0, 0, 0), ("r", 3, 1, 0, 0), ("z", 2, 1, 0, 1),
+        ("r", 2, 0, 1, 0), ("r", 2, 0, 1, 1), ("z", 2, 3, 0, 0), ("z", 3, 3, 0, 1),
+    ),
+    (
+        ("r", 2, 0, 2, 0), ("r", 2, 0, 2, 1), ("z", 2, 2, 0, 1), ("r", 2, 0, 3, 1), ("r", 2, 0, 3, 0),
+    ),
+    (
+
+    ),
+    (
+        ("f", 3, 0, 1, 1), ("z", 3, 1, 1, 0), ("z", 3, 2, 0, 1), ("r", 3, 0, 2, 1), ("f", 3, 0, 3, 0),
+        ("z", 2, 1, 3, 1), ("z", 3, 3, 3, 1), ("z", 3, 3, 1, 1),
+    ),
+    (
+        ("z", 3, 1, 3, 0), ("f", 2, 0, 1, 0), ("r", 3, 0, 2, 0), ("z", 2, 2, 3, 0), ("z", 2, 2, 1, 1),
+        ("f", 2, 0, 2, 0), ("z", 2, 1, 1, 1), ("f", 2, 0, 0, 0), ("r", 3, 1, 2, 1), ("f", 3, 0, 0, 1),
+        ("r", 3, 1, 2, 0), ("f", 3, 1, 0, 0), ("z", 2, 3, 3, 0), ("f", 2, 0, 3, 1), ("z", 3, 1, 2, 0),
+        ("f", 2, 1, 0, 1), ("z", 2, 3, 1, 0),
+    ),
+    (
+
+    ),
+    (
+        ("f", 3, 1, 2, 1), ("f", 3, 0, 2, 0), ("z", 2, 3, 2, 0), ("z", 2, 1, 2, 1), ("z", 3, 3, 2, 1),
+        ("z", 2, 2, 2, 0),
     ),
 )
 
+TURNS = ((1, 0), (1, 0))
 WAVES = [op for part in PLAN for op in part]
 RING_SIDE = {(op[1], op[3]): op[4] for op in WAVES if op[0] == "f" and op[2] == 0}
 RISE = {op[1:4]: op[4] for op in WAVES if op[0] == "z"}
@@ -289,8 +292,9 @@
         return lax.dot_general(H[p][at], tall, NT, preferred_element_type=F32)
 
     def project(b, last, gaps):
-        for p in range(2):
+        for p in TURNS[b]:
             cut = foreign[p]
+            need_all(2 * b + p, False)
             gate_up(b, p, last, False, cut)
             hidden(p, cut)
             PX[b, cut] = down(b, p, cut, other).astype(BF16)
@@ -298,7 +302,7 @@
         for p in range(2):
             PO[foreign[p]] = down(b, p, foreign[p], t)
         gaps[0]()
-        for p in range(2):
+        for p in TURNS[b]:
             cut = foreign[p]
             half_send(b, p).wait_recv()
             S[b, p] = (PO[cut] + PR[b, cut].astype(F32)).astype(BF16)
@@ -338,15 +342,14 @@
         ref = WB[s].at[0:n * depth]
         return lambda key: remote(ref, ref, ws.at[s], wr.at[ARRIVALS[key]], mate)
 
-    def need_all(b, mine):
+    def need_all(s, mine):
         for op in COPIES:
-            if op[1] // 2 == b and own_rows(op) == mine and op in WANTED:
+            if op[1] == s and own_rows(op) == mine and op in WANTED:
                 need(op)
-        for s in (2 * b, 2 * b + 1):
-            key = ("low" if mine else "high", s)
-            n = sum(arrival(op) == key for op in COPIES)
-            if n:
-                slabs(s, n)(key).wait_recv()
+        key = ("low" if mine else "high", s)
+        n = sum(arrival(op) == key for op in COPIES)
+        if n:
+            slabs(s, n)(key).wait_recv()
 
     loaded(0, own_w.at[0])
     loaded(1, pw_ref)
@@ -374,12 +377,11 @@
         mate_send(0, p).wait_recv()
         norm_rows(0, foreign[p])
     issue(4)
-    need_all(0, True)
-    for p in range(2):
+    for p in TURNS[0]:
+        need_all(p, True)
         gate_up(0, p, low, True, foreign[p])
         gate_up(0, p, low, True, own)
     issue(5)
-    need_all(0, False)
     first = project(0, high, [lambda: issue(6), lambda: issue(7), ready_pool])
 
     after_first = (TB[0, t, own].astype(F32) + 0.5 * first).astype(BF16).astype(F32)
@@ -421,14 +423,13 @@
     for p in range(2):
         tok_here(1, p)
         mate_send(1, p).start()
-    need_all(1, True)
-    for p in range(2):
+    for p in TURNS[1]:
+        need_all(2 + p, True)
         gate_up(1, p, low, True, own)
-    for p in range(2):
+    for p in TURNS[1]:
         mate_send(1, p).wait_recv()
         norm_rows(1, foreign[p])
         gate_up(1, p, low, True, foreign[p])
-    need_all(1, False)
     second = project(1, high, [lambda: None] * 3)
     out_ref[...] = (TB[1, t, own].astype(F32) + 0.5 * second).astype(BF16)
 
@@ -460,7 +461,7 @@
     dma = pltpu.SemaphoreType.DMA
     out = pl.pallas_call(
         layer_kernel,
-        out_shape=jax.ShapeDtypeStruct((rows, half), BF16),
+        out_shape=pltpu.VMEM((rows, half), BF16),
         in_specs=[anyw] * 12,
         out_specs=vmem,
         scratch_shapes=[

time: 63.5 us -> 60.5 us (0.953)
  Pallas kernels: 61.7 us -> 59.7 us
  local copies, waits for them, and re-layouts: 1.67 us -> 0.71 us
    pallas_call x1, Pallas kernels: 61.7 us -> 59.7 us  [fused(): pl.pallas_call(layer_kernel, out_shape=pltpu.VMEM((rows, half), BF16), in...]
    unnamed x1, local copies, waits for them, and re-layouts: 1.67 us -> 0.71 us
where the time goes in v6:
time: 60.5 us; the launch traced here: 60.4 us
  Pallas kernels  59.7 us (99%)
  local copies, waits for them, and re-layouts  0.71 us (1%)
    pallas_call x1, Pallas kernels, fused(): pl.pallas_call(layer_kernel, out_shape=pltpu.VMEM((rows, half), BF16), in...  59.7 us

profile of v6, /device:TPU:1, one launch (start us, length us, event | category | flops | bytes accessed | tf_op | source)
XLA Modules:
  0.0 60.4 jit_solution(17290065229292744858)
XLA Ops:
  0.0 59.7 %shard_map.118 = bf16[256,512]{1,0:T(8,128)(2,1)S(1)} custom-call(bf16[256,512]{1,0:T(8,128)(2,1)} %bitcast.12, f32[1,1024]{1,0:T(1,128)} %bitcast.16, f32[1,512]{1,0:T(1,128)} %bitcast.18, f32[1,512]{1,0:T(1,128)} %bitcast.19, f32[1,1024]{1,0:T(1,128)} %bitcast.17, bf16[16,256]{1,0:T(8,128)(2,1)} %bitcast.15, bf16[32,1280]{1,0:T(8,128)(2,1)} %g1_hbm.1, ...), custom_call_target="tpu_custom_call" | custom-call | tf_op jit(solution)/shard_map/pallas_call | solution.py:462
  59.7 0.7 %copy.14 = bf16[1,256,512]{2,1,0:T(8,128)(2,1)} copy(bf16[1,256,512]{2,1,0:T(8,128)(2,1)S(1)} %bitcast.11) | data formatting | bytes 524288

commit v7 on v6

--- a/solution.py
+++ b/solution.py
@@ -66,7 +66,7 @@
     ),
 )
 
-TURNS = ((1, 0), (1, 0))
+TURNS = ((1, 0), (0, 1))
 WAVES = [op for part in PLAN for op in part]
 RING_SIDE = {(op[1], op[3]): op[4] for op in WAVES if op[0] == "f" and op[2] == 0}
 RISE = {op[1:4]: op[4] for op in WAVES if op[0] == "z"}
@@ -108,7 +108,7 @@
     tok_hbm, pre_hbm, mixg_hbm, scale_hbm, post_hbm, pw_hbm,
     g1_hbm, u1_hbm, d1_hbm, g2_hbm, u2_hbm, d2_hbm, out_ref,
     wide_gain, slim_gain, pw_ref, own_w,
-    WS0, WS1, WS2, WS3, WB0, WB1, WB2, WB3, TB, N, ACC0, ACC1, H0, H1, PX, PR, PO, S, R, SQ, TM, RC,
+    WS0, WS1, WS2, WS3, WB0, WB1, WB2, WB3, TB, N, ACC0, ACC1, H0, H1, PX, PR, PO, S, R, SQ, TM, RC, HB,
     ls, ws, wr, ts, tr, ms, mr, hs, hr, rs, rr, qs,
 ):
     rep = lax.axis_index("rep")
@@ -196,8 +196,6 @@
 
     def copy_of(op):
         kind = op[0]
-        if kind == "t":
-            return tok_send(0, op[1], op[2])
         s = op[1]
         axis, ring = axes[turn[s]], axes[1 - turn[s]]
         sems = (ws.at[s], wr.at[ARRIVALS[arrival(op)]])
@@ -228,7 +226,11 @@
         for op in PLAN[part]:
             for source in sources(op):
                 need(source)
-            copy_of(op).start()
+            if op[0] == "t":
+                for k in range(2):
+                    tok_send(0, op[1], op[2], k).start()
+            else:
+                copy_of(op).start()
 
     def base(p):
         return rows * (1 + p)
@@ -239,29 +241,40 @@
     def axis_of(b, p):
         return axes[turn[2 * b + p]]
 
-    def tok_send(b, p, i):
-        src = TB.at[b, t, i * piece:(i + 1) * piece]
-        dst = TB.at[b, t, base(p) + i * piece:base(p) + (i + 1) * piece]
-        return remote(src, dst, ts.at[b], tr.at[b, p], axis_of(b, p)[(1, 3)[i]])
-
-    def tok_here(b, p):
-        ref = TB.at[b, t, foreign[p]]
-        remote(ref, ref, ts.at[b], tr.at[b, p], mate).wait_recv()
-
-    def mate_send(b, n):
-        ref = TB.at[b, t, own if n == 2 else foreign[n]]
+    def part_of(k):
+        return slice(k * piece, (k + 1) * piece)
+
+    def far_part(p, k):
+        return slice(base(p) + k * piece, base(p) + (k + 1) * piece)
+
+    def strip(i, k):
+        return slice(k * piece + i * piece // 2, k * piece + (i + 1) * piece // 2)
+
+    def tok_send(b, p, i, k):
+        cut = strip(i, k)
+        src = TB.at[b, t, cut]
+        dst = TB.at[b, t, base(p) + cut.start:base(p) + cut.stop]
+        return remote(src, dst, ts.at[b], tr.at[b, p, k * b], axis_of(b, p)[(1, 3)[i]])
+
+    def tok_here(b, p, k, cut):
+        ref = TB.at[b, t, cut]
+        remote(ref, ref, ts.at[b], tr.at[b, p, k], mate).wait_recv()
+
+    def mate_send(b, n, cut):
+        ref = TB.at[b, t, cut]
         return remote(ref, ref, ms.at[b], mr.at[b, n], mate)
 
     def half_send(b, n):
         cut = own if n == 2 else foreign[n]
         return remote(PX.at[b, cut], PR.at[b, cut], hs.at[b], hr.at[b, n], mate)
 
-    def back_send(b, p, i):
-        cut = slice(i * piece, (i + 1) * piece)
-        return remote(S.at[b, p, cut], R.at[b, p, cut], rs.at[b], rr.at[b, p], axis_of(b, p)[(3, 1)[i]])
-
-    def back_here(b, p):
-        remote(S.at[b, p], R.at[b, p], rs.at[b], rr.at[b, p], mate).wait_recv()
+    def back_send(b, p, i, k):
+        cut = strip(i, k)
+        return remote(S.at[b, p, cut], R.at[b, p, cut], rs.at[b], rr.at[b, p, k], axis_of(b, p)[(3, 1)[i]])
+
+    def back_here(b, p, k):
+        cut = part_of(k)
+        remote(S.at[b, p, cut], R.at[b, p, cut], rs.at[b], rr.at[b, p, k], mate).wait_recv()
 
     def norm_rows(b, cut):
         parts = [TB[b, c, cut].astype(F32) for c in range(2)]
@@ -270,20 +283,14 @@
         for c in range(2):
             N[c, cut] = (parts[c] * inv * wide_gain[b:b + 1, c * half:(c + 1) * half]).astype(BF16)
 
-    def gate_up(b, p, lo, fresh, cut):
-        n = 2 * widths[p]
-        wide = side_of(2 * b + p, lo, slice(0, n))
-        value = jnp.dot(N[lo, cut], wide, preferred_element_type=F32)
-        at = own if cut is own else slice(rows, 2 * rows)
-        if fresh:
-            ACC[p][at] = value
-        else:
-            ACC[p][at] += value
-
-    def hidden(p, cut):
+    def gate_up(b, p, lo, cut):
+        wide = side_of(2 * b + p, lo, slice(0, 2 * widths[p]))
+        return jnp.dot(N[lo, cut], wide, preferred_element_type=F32)
+
+    def hidden(p, cut, value):
         at = own if cut is own else slice(rows, 2 * rows)
         n = widths[p]
-        H[p][at] = (jax.nn.silu(ACC[p][at, 0:n]) * ACC[p][at, n:2 * n]).astype(BF16)
+        H[p][at] = (jax.nn.silu(value[:, 0:n]) * value[:, n:2 * n]).astype(BF16)
 
     def down(b, p, cut, lo):
         at = own if cut is own else slice(rows, 2 * rows)
@@ -291,12 +298,12 @@
         tall = side_of(2 * b + p, lo, slice(2 * n, 3 * n))
         return lax.dot_general(H[p][at], tall, NT, preferred_element_type=F32)
 
-    def project(b, last, gaps):
+    def project(b, gaps):
         for p in TURNS[b]:
             cut = foreign[p]
             need_all(2 * b + p, False)
-            gate_up(b, p, last, False, cut)
-            hidden(p, cut)
+            begun = ACC[p][...] if b == 0 else gate_up(b, p, low, cut)
+            hidden(p, cut, begun + gate_up(b, p, high, cut))
             PX[b, cut] = down(b, p, cut, other).astype(BF16)
             half_send(b, p).start()
         for p in range(2):
@@ -306,21 +313,24 @@
             cut = foreign[p]
             half_send(b, p).wait_recv()
             S[b, p] = (PO[cut] + PR[b, cut].astype(F32)).astype(BF16)
-            for i in range(2):
-                back_send(b, p, i).start()
+            for k in range(2):
+                for i in range(2):
+                    back_send(b, p, i, k).start()
         for p in range(2):
-            gate_up(b, p, last, False, own)
-            hidden(p, own)
+            hidden(p, own, gate_up(b, p, low, own) + gate_up(b, p, high, own))
         PX[b, own] = (down(b, 0, own, other) + down(b, 1, own, other)).astype(BF16)
         half_send(b, 2).start()
         gaps[1]()
         PO[own] = down(b, 0, own, t) + down(b, 1, own, t)
         gaps[2]()
         half_send(b, 2).wait_recv()
-        total = PO[own] + PR[b, own].astype(F32)
+
+    def collect(b, k):
+        cut = part_of(k)
+        total = PO[cut] + PR[b, cut].astype(F32)
         for p in range(2):
-            back_here(b, p)
-            total = total + R[b, p].astype(F32)
+            back_here(b, p, k)
+            total = total + R[b, p, cut].astype(F32)
         return total
 
     groups_here = 2
@@ -364,85 +374,94 @@
     pl.semaphore_wait(barrier, len(peers))
 
     issue(0)
-    mate_send(0, 2).start()
-    mate_send(0, 2).wait_recv()
+    mate_send(0, 2, own).start()
+    mate_send(0, 2, own).wait_recv()
     norm_rows(0, own)
     issue(1)
     issue(2)
     for p in range(2):
-        tok_here(0, p)
-        mate_send(0, p).start()
+        tok_here(0, p, 0, foreign[p])
+        mate_send(0, p, foreign[p]).start()
     issue(3)
     for p in range(2):
-        mate_send(0, p).wait_recv()
+        mate_send(0, p, foreign[p]).wait_recv()
         norm_rows(0, foreign[p])
     issue(4)
     for p in TURNS[0]:
         need_all(p, True)
-        gate_up(0, p, low, True, foreign[p])
-        gate_up(0, p, low, True, own)
+        ACC[p][...] = gate_up(0, p, low, foreign[p])
     issue(5)
-    first = project(0, high, [lambda: issue(6), lambda: issue(7), ready_pool])
-
-    after_first = (TB[0, t, own].astype(F32) + 0.5 * first).astype(BF16).astype(F32)
-    square = after_first * after_first
-    SQ[0] = sum(square[:, i * 128:(i + 1) * 128] for i in range(half // 128))
-    swap = remote(SQ.at[0], SQ.at[1], qs.at[0], qs.at[1], mate)
-    swap.start()
-    swap.wait_recv()
-    total = jnp.sum(SQ[0] + SQ[1], axis=-1, keepdims=True)
-    h = (after_first * lax.rsqrt(total / (2 * half) + epsilon) * slim_gain[0:1, :]).astype(BF16).astype(F32)
+    project(0, [lambda: issue(6), lambda: issue(7), ready_pool])
 
     def shifted(v, by):
         spot_ids = lax.broadcasted_iota(jnp.int32, v.shape, 0)
         return jnp.where(spot_ids >= by, pltpu.roll(v, by, 0), 0.0)
 
-    for g in range(groups_here):
-        hg = h[:, g * width:(g + 1) * width]
-        run = hg + shifted(hg, 1)
-        window = 2
-        found = run
-        number = t * groups_here + g
-        for level in range(1, GROUPS):
-            run = run + shifted(run, window)
-            window = window * 2
-            found = jnp.where(number >= level, run, found)
-        share = jnp.concatenate([RC[g]] * (width // 128), axis=1)
-        diff = (found * share - hg).astype(BF16)
-        mixed = lax.dot_general(diff, TM[g], NT, preferred_element_type=F32)
-        at = slice(g * width, (g + 1) * width)
-        TB[1, t, own, at] = (after_first[:, at] + slim_gain[1:2, at] * mixed).astype(BF16)
-
-    for p in range(2):
-        for i in range(2):
-            tok_send(1, p, i).start()
-    mate_send(1, 2).start()
-    mate_send(1, 2).wait_recv()
-    norm_rows(1, own)
+    def swap(k):
+        cut = part_of(k)
+        return remote(SQ.at[0, cut], SQ.at[1, cut], qs.at[0], qs.at[1 + k], mate)
+
+    reach = 2 ** GROUPS
+    for k in range(2):
+        cut = part_of(k)
+        after_first = (TB[0, t, cut].astype(F32) + 0.5 * collect(0, k)).astype(BF16).astype(F32)
+        square = after_first * after_first
+        SQ[0, cut] = sum(square[:, i * 128:(i + 1) * 128] for i in range(half // 128))
+        swap(k).start()
+        swap(k).wait_recv()
+        total = jnp.sum(SQ[0, cut] + SQ[1, cut], axis=-1, keepdims=True)
+        inv = lax.rsqrt(total / (2 * half) + epsilon)
+        HB[cut] = (after_first * inv * slim_gain[0:1, :]).astype(BF16).astype(F32)
+        lead = reach if k else 0
+        for g in range(groups_here):
+            at = slice(g * width, (g + 1) * width)
+            hg = HB[cut.start - lead:cut.stop, at]
+            run = hg + shifted(hg, 1)
+            window = 2
+            found = run
+            number = t * groups_here + g
+            for level in range(1, GROUPS):
+                run = run + shifted(run, window)
+                window = window * 2
+                found = jnp.where(number >= level, run, found)
+            share = jnp.concatenate([RC[g, cut]] * (width // 128), axis=1)
+            diff = (found[lead:] * share - hg[lead:]).astype(BF16)
+            mixed = lax.dot_general(diff, TM[g], NT, preferred_element_type=F32)
+            TB[1, t, cut, at] = (after_first[:, at] + slim_gain[1:2, at] * mixed).astype(BF16)
+        for p in range(2):
+            for i in range(2):
+                tok_send(1, p, i, k).start()
+        mate_send(1, 2 + 3 * k, cut).start()
+
     issue(9)
-    for p in range(2):
-        tok_here(1, p)
-        mate_send(1, p).start()
+    for k in range(2):
+        for p in TURNS[1]:
+            tok_here(1, p, k, far_part(p, k))
+            mate_send(1, p + 3 * k, far_part(p, k)).start()
+        if k == 0:
+            for i in range(2):
+                mate_send(1, 2 + 3 * i, part_of(i)).wait_recv()
+            norm_rows(1, own)
+        for p in TURNS[1]:
+            mate_send(1, p + 3 * k, far_part(p, k)).wait_recv()
+            norm_rows(1, far_part(p, k))
     for p in TURNS[1]:
         need_all(2 + p, True)
-        gate_up(1, p, low, True, own)
-    for p in TURNS[1]:
-        mate_send(1, p).wait_recv()
-        norm_rows(1, foreign[p])
-        gate_up(1, p, low, True, foreign[p])
-    second = project(1, high, [lambda: None] * 3)
-    out_ref[...] = (TB[1, t, own].astype(F32) + 0.5 * second).astype(BF16)
+    project(1, [lambda: None] * 3)
+    for k in range(2):
+        cut = part_of(k)
+        out_ref[cut] = (TB[1, t, cut].astype(F32) + 0.5 * collect(1, k)).astype(BF16)
 
     for s in range(4):
         n = sum(op[1] == s for op in COPIES)
         ref = WB[s].at[0:n * depth]
         remote(ref, ref, ws.at[s], wr.at[0], mate).wait_send()
     for b in range(2):
-        remote(S.at[b], R.at[b], ts.at[b], tr.at[b, 0], mate).wait_send()
-        remote(S.at[b], R.at[b], rs.at[b], rr.at[b, 0], mate).wait_send()
+        remote(S.at[b], R.at[b], ts.at[b], tr.at[b, 0, 0], mate).wait_send()
+        remote(S.at[b], R.at[b], rs.at[b], rr.at[b, 0, 0], mate).wait_send()
         remote(PX.at[b], PR.at[b], ms.at[b], mr.at[b, 0], mate).wait_send()
         remote(PX.at[b], PR.at[b], hs.at[b], hr.at[b, 0], mate).wait_send()
-    swap.wait_send()
+    remote(SQ.at[0], SQ.at[1], qs.at[0], qs.at[1], mate).wait_send()
 
 
 def fused(
@@ -475,8 +494,8 @@
         + [
             pltpu.VMEM((2, 2, 3 * rows, half), BF16),
             pltpu.VMEM((2, 3 * rows, half), BF16),
-            pltpu.VMEM((2 * rows, 2 * wide), F32),
-            pltpu.VMEM((2 * rows, 2 * slim), F32),
+            pltpu.VMEM((rows, 2 * wide), F32),
+            pltpu.VMEM((rows, 2 * slim), F32),
             pltpu.VMEM((2 * rows, wide), BF16),
             pltpu.VMEM((2 * rows, slim), BF16),
             pltpu.VMEM((2, 3 * rows, half), BF16),
@@ -487,9 +506,10 @@
             pltpu.VMEM((2, rows, 128), F32),
             pltpu.VMEM((groups, width, width), BF16),
             pltpu.VMEM((groups, rows, 128), F32),
+            pltpu.VMEM((rows, half), F32),
             dma((6,)), dma((4,)), dma((len(ARRIVALS),)),
-            dma((2,)), dma((2, 2)), dma((2,)), dma((2, 3)), dma((2,)), dma((2, 3)),
-            dma((2,)), dma((2, 2)), dma((2,)),
+            dma((2,)), dma((2, 2, 2)), dma((2,)), dma((2, 6)), dma((2,)), dma((2, 3)),
+            dma((2,)), dma((2, 2, 2)), dma((3,)),
         ],
         compiler_params=pltpu.CompilerParams(
             collective_id=0, has_side_effects=True, vmem_limit_bytes=60 * 1024 * 1024

time: 60.5 us -> 57.8 us (0.955)
  Pallas kernels: 59.7 us -> 56.9 us
    pallas_call x1, Pallas kernels: 59.7 us -> 56.9 us  [fused(): pl.pallas_call(layer_kernel, out_shape=pltpu.VMEM((rows, half), BF16), in...]
where the time goes in v7:
time: 57.8 us; the launch traced here: 57.6 us
  Pallas kernels  56.9 us (98%)
  local copies, waits for them, and re-layouts  0.71 us (1%)
    pallas_call x1, Pallas kernels, fused(): pl.pallas_call(layer_kernel, out_shape=pltpu.VMEM((rows, half), BF16), in...  56.9 us

profile of v7, /device:TPU:1, one launch (start us, length us, event | category | flops | bytes accessed | tf_op | source)
XLA Modules:
  0.0 57.6 jit_solution(4708005680286268767)
XLA Ops:
  0.0 56.9 %shard_map.118 = bf16[256,512]{1,0:T(8,128)(2,1)S(1)} custom-call(bf16[256,512]{1,0:T(8,128)(2,1)} %bitcast.12, f32[1,1024]{1,0:T(1,128)} %bitcast.16, f32[1,512]{1,0:T(1,128)} %bitcast.18, f32[1,512]{1,0:T(1,128)} %bitcast.19, f32[1,1024]{1,0:T(1,128)} %bitcast.17, bf16[16,256]{1,0:T(8,128)(2,1)} %bitcast.15, bf16[32,1280]{1,0:T(8,128)(2,1)} %g1_hbm.1, ...), custom_call_target="tpu_custom_call" | custom-call | tf_op jit(solution)/shard_map/pallas_call | solution.py:481
  56.9 0.7 %copy.14 = bf16[1,256,512]{2,1,0:T(8,128)(2,1)} copy(bf16[1,256,512]{2,1,0:T(8,128)(2,1)S(1)} %bitcast.11) | data formatting | bytes 524288

commit v8 on v7

--- a/solution.py
+++ b/solution.py
@@ -16,52 +16,51 @@
 PLAN = (
     (
         ("c", 0, 1), ("c", 1, 3), ("c", 1, 1), ("c", 0, 3), ("z", 0, 0, 0, 1), ("z", 1, 0, 0, 0), ("c", 1, 2),
-        ("z", 3, 0, 0, 0), ("c", 0, 2), ("z", 2, 0, 0, 1), ("r", 0, 0, 0, 1), ("t", 1, 0), ("r", 1, 0, 0, 0),
-        ("r", 1, 0, 0, 1),
-    ),
-    (
-        ("z", 1, 3, 0, 1), ("z", 1, 1, 0, 0), ("r", 1, 0, 3, 0), ("r", 1, 0, 3, 1), ("r", 1, 0, 1, 0),
+        ("z", 3, 0, 0, 0), ("c", 0, 2), ("z", 2, 0, 0, 1), ("r", 0, 0, 0, 1), ("t", 1, 0), ("r", 1, 0, 0, 1),
+        ("t", 0, 0),
+    ),
+    (
+        ("z", 1, 3, 0, 1), ("z", 1, 1, 0, 0), ("r", 1, 0, 3, 1), ("r", 1, 0, 3, 0), ("r", 1, 0, 1, 0),
         ("r", 0, 0, 3, 1), ("z", 0, 3, 0, 0), ("z", 0, 1, 0, 1), ("r", 0, 0, 1, 0), ("r", 0, 0, 1, 1),
-        ("r", 1, 0, 2, 1), ("z", 1, 2, 0, 0), ("r", 1, 0, 1, 1), ("r", 1, 0, 2, 0), ("r", 1, 1, 0, 0),
-        ("r", 1, 1, 0, 1), ("z", 0, 2, 0, 1), ("r", 0, 0, 2, 0), ("r", 0, 0, 2, 1), ("r", 0, 0, 3, 0),
-        ("r", 0, 1, 0, 0), ("f", 1, 0, 0, 1), ("z", 0, 3, 1, 0), ("z", 1, 3, 3, 1), ("f", 0, 0, 3, 1),
-        ("z", 1, 3, 1, 1), ("f", 1, 0, 3, 0), ("r", 0, 1, 0, 1), ("t", 1, 1), ("z", 1, 1, 3, 0),
-        ("z", 1, 2, 3, 1), ("f", 1, 0, 2, 0), ("f", 1, 0, 1, 1), ("z", 1, 1, 1, 0), ("z", 0, 1, 1, 1),
-        ("t", 0, 1), ("c", 3, 1), ("r", 2, 0, 0, 1), ("r", 2, 1, 0, 1), ("f", 0, 0, 2, 0), ("z", 0, 2, 3, 0),
-        ("f", 0, 0, 1, 0), ("r", 0, 0, 0, 0), ("c", 2, 3),
-    ),
-    (
-        ("f", 1, 1, 0, 0), ("t", 0, 0), ("c", 3, 3), ("r", 2, 0, 0, 0), ("r", 2, 1, 0, 0), ("c", 3, 2),
-        ("z", 0, 3, 3, 0), ("z", 1, 3, 2, 1), ("z", 0, 2, 1, 1), ("z", 1, 1, 2, 0), ("z", 1, 2, 2, 1),
-        ("z", 0, 3, 2, 0), ("z", 1, 2, 1, 0), ("f", 0, 1, 0, 1), ("c", 2, 1), ("c", 2, 2), ("z", 0, 2, 2, 0),
-        ("z", 0, 1, 2, 1), ("z", 0, 1, 3, 1), ("z", 3, 1, 0, 0),
-    ),
-    (
-        ("f", 0, 0, 0, 0), ("r", 3, 0, 3, 1), ("r", 3, 0, 1, 1), ("r", 3, 0, 3, 0), ("r", 3, 1, 0, 1),
-        ("r", 3, 0, 1, 0), ("r", 3, 0, 0, 1), ("r", 3, 0, 0, 0), ("r", 3, 1, 0, 0), ("z", 2, 1, 0, 1),
-        ("r", 2, 0, 1, 0), ("r", 2, 0, 1, 1), ("z", 2, 3, 0, 0), ("z", 3, 3, 0, 1),
-    ),
-    (
-        ("r", 2, 0, 2, 0), ("r", 2, 0, 2, 1), ("z", 2, 2, 0, 1), ("r", 2, 0, 3, 1), ("r", 2, 0, 3, 0),
-    ),
-    (
-
-    ),
-    (
-        ("f", 3, 0, 1, 1), ("z", 3, 1, 1, 0), ("z", 3, 2, 0, 1), ("r", 3, 0, 2, 1), ("f", 3, 0, 3, 0),
-        ("z", 2, 1, 3, 1), ("z", 3, 3, 3, 1), ("z", 3, 3, 1, 1),
-    ),
-    (
-        ("z", 3, 1, 3, 0), ("f", 2, 0, 1, 0), ("r", 3, 0, 2, 0), ("z", 2, 2, 3, 0), ("z", 2, 2, 1, 1),
-        ("f", 2, 0, 2, 0), ("z", 2, 1, 1, 1), ("f", 2, 0, 0, 0), ("r", 3, 1, 2, 1), ("f", 3, 0, 0, 1),
-        ("r", 3, 1, 2, 0), ("f", 3, 1, 0, 0), ("z", 2, 3, 3, 0), ("f", 2, 0, 3, 1), ("z", 3, 1, 2, 0),
-        ("f", 2, 1, 0, 1), ("z", 2, 3, 1, 0),
-    ),
-    (
-
-    ),
-    (
-        ("f", 3, 1, 2, 1), ("f", 3, 0, 2, 0), ("z", 2, 3, 2, 0), ("z", 2, 1, 2, 1), ("z", 3, 3, 2, 1),
+        ("r", 1, 0, 2, 1), ("z", 1, 2, 0, 0), ("r", 1, 0, 1, 1), ("r", 1, 1, 0, 1), ("r", 1, 0, 2, 0),
+        ("r", 1, 1, 0, 0), ("z", 0, 2, 0, 1), ("r", 0, 0, 2, 0), ("r", 0, 0, 2, 1), ("r", 0, 0, 3, 0),
+        ("f", 1, 0, 0, 1), ("z", 0, 3, 1, 0), ("z", 1, 3, 1, 1), ("f", 0, 0, 3, 1), ("r", 0, 1, 0, 1),
+        ("t", 1, 1), ("z", 0, 1, 3, 1), ("f", 0, 0, 1, 0), ("z", 1, 2, 1, 0), ("f", 1, 0, 3, 0),
+        ("z", 0, 1, 1, 1), ("f", 1, 0, 1, 1), ("z", 1, 1, 1, 0), ("t", 0, 1), ("c", 3, 1), ("r", 2, 0, 0, 1),
+        ("r", 2, 1, 0, 1), ("f", 0, 0, 2, 0), ("z", 1, 1, 3, 0), ("r", 0, 0, 0, 0), ("r", 0, 1, 0, 0),
+    ),
+    (
+        ("f", 1, 0, 2, 0), ("z", 1, 2, 3, 1), ("r", 1, 0, 0, 0), ("z", 0, 2, 1, 1), ("z", 0, 3, 3, 0),
+        ("f", 1, 1, 0, 0), ("c", 3, 3), ("r", 2, 0, 0, 0), ("r", 2, 1, 0, 0), ("c", 3, 2), ("z", 0, 1, 2, 1),
+        ("z", 1, 1, 2, 0), ("z", 0, 3, 2, 0), ("z", 0, 2, 3, 0), ("f", 0, 1, 0, 1), ("c", 2, 2), ("c", 2, 1),
+        ("z", 1, 3, 2, 1), ("z", 1, 3, 3, 1), ("z", 0, 2, 2, 0), ("z", 1, 2, 2, 1), ("f", 0, 0, 0, 0),
+        ("c", 2, 3),
+    ),
+    (
+        ("z", 3, 1, 0, 0), ("r", 3, 0, 3, 1), ("z", 3, 3, 0, 1), ("r", 3, 0, 1, 1), ("r", 3, 0, 3, 0),
+        ("r", 3, 1, 0, 1), ("r", 3, 0, 1, 0), ("r", 3, 0, 0, 1), ("r", 3, 0, 0, 0), ("r", 3, 1, 0, 0),
+    ),
+    (
+        ("r", 2, 0, 2, 0), ("r", 2, 0, 2, 1), ("z", 2, 2, 0, 1), ("r", 2, 0, 1, 0), ("r", 2, 0, 1, 1),
+    ),
+    (
+        ("z", 3, 3, 1, 1), ("z", 2, 3, 0, 0), ("r", 2, 0, 3, 1), ("r", 2, 0, 3, 0),
+    ),
+    (
+        ("f", 3, 0, 1, 1), ("z", 3, 1, 1, 0), ("z", 3, 2, 0, 1), ("r", 3, 0, 2, 1), ("z", 3, 3, 3, 1),
+        ("f", 3, 0, 3, 0), ("z", 2, 1, 0, 1), ("z", 2, 2, 3, 0),
+    ),
+    (
+        ("z", 2, 1, 1, 1), ("z", 2, 1, 3, 1), ("z", 2, 2, 1, 1), ("f", 2, 0, 1, 0), ("f", 2, 0, 2, 0),
+        ("f", 2, 0, 0, 0), ("z", 3, 1, 2, 0), ("r", 3, 1, 2, 1), ("f", 3, 0, 0, 1), ("r", 3, 0, 2, 0),
+        ("r", 3, 1, 2, 0), ("f", 3, 1, 0, 0), ("f", 2, 0, 3, 1), ("z", 2, 3, 3, 0), ("f", 2, 1, 0, 1),
+        ("z", 2, 3, 1, 0), ("z", 3, 1, 3, 0),
+    ),
+    (
+
+    ),
+    (
+        ("f", 3, 1, 2, 1), ("z", 2, 1, 2, 1), ("z", 2, 3, 2, 0), ("z", 3, 3, 2, 1), ("f", 3, 0, 2, 0),
         ("z", 2, 2, 2, 0),
     ),
 )

time: 57.8 us -> 57.4 us (level)
  no operation moved by 1% of the time
where the time goes in v8:
time: 57.4 us; the launch traced here: 57.2 us
  Pallas kernels  56.5 us (98%)
  local copies, waits for them, and re-layouts  0.71 us (1%)
    pallas_call x1, Pallas kernels, fused(): pl.pallas_call(layer_kernel, out_shape=pltpu.VMEM((rows, half), BF16), in...  56.5 us

profile of v8, /device:TPU:1, one launch (start us, length us, event | category | flops | bytes accessed | tf_op | source)
XLA Modules:
  0.0 57.2 jit_solution(15829743655421620974)
XLA Ops:
  0.0 56.5 %shard_map.118 = bf16[256,512]{1,0:T(8,128)(2,1)S(1)} custom-call(bf16[256,512]{1,0:T(8,128)(2,1)} %bitcast.12, f32[1,1024]{1,0:T(1,128)} %bitcast.16, f32[1,512]{1,0:T(1,128)} %bitcast.18, f32[1,512]{1,0:T(1,128)} %bitcast.19, f32[1,1024]{1,0:T(1,128)} %bitcast.17, bf16[16,256]{1,0:T(8,128)(2,1)} %bitcast.15, bf16[32,1280]{1,0:T(8,128)(2,1)} %g1_hbm.1, ...), custom_call_target="tpu_custom_call" | custom-call | tf_op jit(solution)/shard_map/pallas_call | solution.py:480
  56.5 0.7 %copy.14 = bf16[1,256,512]{2,1,0:T(8,128)(2,1)} copy(bf16[1,256,512]{2,1,0:T(8,128)(2,1)S(1)} %bitcast.11) | data formatting | bytes 524288

commit v9 on v8

--- a/solution.py
+++ b/solution.py
@@ -130,7 +130,7 @@
     along_x = {d: dev(d, 0, 0, t) for d in (1, 2, 3)}
     along_y = {d: dev(0, d, 0, t) for d in (1, 2, 3)}
     along_z = {d: dev(0, 0, d, t) for d in (1, 3)}
-    peers = [mate] + list(along_x.values()) + list(along_y.values()) + list(along_z.values())
+    peers = [along_x[2], along_y[2]] + [axis[d] for axis in (along_x, along_y, along_z) for d in (1, 3)] + [mate]
 
     barrier = pltpu.get_barrier_semaphore()
     for peer in peers:

time: 57.4 us -> 57.4 us (level)
  no operation moved by 1% of the time
where the time goes in v9:
time: 57.4 us; the launch traced here: 57.2 us
  Pallas kernels  56.5 us (98%)
  local copies, waits for them, and re-layouts  0.71 us (1%)
    pallas_call x1, Pallas kernels, fused(): pl.pallas_call(layer_kernel, out_shape=pltpu.VMEM((rows, half), BF16), in...  56.5 us

profile of v9, /device:TPU:1, one launch (start us, length us, event | category | flops | bytes accessed | tf_op | source)
XLA Modules:
  0.0 57.2 jit_solution(9114961445456515693)
XLA Ops:
  0.0 56.5 %shard_map.118 = bf16[256,512]{1,0:T(8,128)(2,1)S(1)} custom-call(bf16[256,512]{1,0:T(8,128)(2,1)} %bitcast.12, f32[1,1024]{1,0:T(1,128)} %bitcast.16, f32[1,512]{1,0:T(1,128)} %bitcast.18, f32[1,512]{1,0:T(1,128)} %bitcast.19, f32[1,1024]{1,0:T(1,128)} %bitcast.17, bf16[16,256]{1,0:T(8,128)(2,1)} %bitcast.15, bf16[32,1280]{1,0:T(8,128)(2,1)} %g1_hbm.1, ...), custom_call_target="tpu_custom_call" | custom-call | tf_op jit(solution)/shard_map/pallas_call | solution.py:480
  56.5 0.7 %copy.14 = bf16[1,256,512]{2,1,0:T(8,128)(2,1)} copy(bf16[1,256,512]{2,1,0:T(8,128)(2,1)S(1)} %bitcast.11) | data formatting | bytes 524288
